TPU v7x, 32 devices: a whole 2x2x4 slice. The times are simulated.
32 devices in a mesh: fs: 4 (over z), rep: 4 (over y, x), tp: 2 (over core).
Axes of the slice: x: 2, y: 2, z: 4, core: 2. Of those that a mesh axis runs over, the one named last changes fastest.
Arguments:
- mixer_out: bfloat16 [16384, 1536], P(('fs', 'rep')), may hold values from -6 to 6
- out_grad: bfloat16 [16384, 4096], P(('fs', 'rep'), 'tp'), may hold values from -0.046875 to 0.046875
- factors: bfloat16 [1536, 256], P(('fs', 'rep')), may hold values from -0.15625 to 0.15625
- weight: float32 [1536, 4096], P(('fs', 'rep'), 'tp'), may hold values from -0.15625 to 0.15625
- first_moment: float32 [256, 4096], P(('fs', 'rep'), 'tp'), may hold values from -6 to 6
- second_moment: float32 [256, 4096], P(('fs', 'rep'), 'tp'), may hold values from 0.05 to 2
Outputs:
- new_weight: float32 [1536, 4096], P(('fs', 'rep'), 'tp')
- update: float32 [1536, 4096], P(('fs', 'rep'), 'tp')
- new_first: float32 [256, 4096], P(('fs', 'rep'), 'tp')
- new_second: float32 [256, 4096], P(('fs', 'rep'), 'tp')
- weight_copy: bfloat16 [1536, 4096], P(None, 'tp')
All inputs are finite; a program needn't handle non-finite values.
Results may differ from a plain program's by a relative error of at most 0.0034.
Values may be sent and summed in bfloat16 or wider, within the bound.
A program may use at most 64 MiB of HBM per device.

v0:
```python
import functools

import jax
import jax.numpy as jnp
from jax import lax
from jax.experimental import pallas as pl
from jax.experimental.pallas import tpu as pltpu
from jax.sharding import PartitionSpec as P

MESH = pl.DeviceIdType.MESH
LANES = 128
TILE = 256


def contract_rows(left, right):
    return lax.dot_general(
        left, right, (((0,), (0,)), ((), ())), preferred_element_type=jnp.float32
    )


def fused_kernel(
    Z, R, T,
    m_ref, o_ref, f_ref, w_ref, m1_ref, m2_ref,
    nw_ref, upd_ref, nf_ref, ns_ref, wc_ref,
    mt, send1, recv1, own, send2, recv2, grad, f_all, m1_all, m2_all,
    nf_col, ns_col, upd_col, stat, stat_all,
    s1_send, s1_recv, s2_send, s2_recv,
    fa_send, fa_recv, ma_send, ma_recv, mb_send, mb_recv,
    st_send, st_recv, nf_send, nf_recv, ns_send, ns_recv, up_send, up_recv,
    gz_send, gz_recv, gr_send, gr_recv,
    recvd, d_send, d_recv, gh_send, gh_recv,
):
    N = Z * R
    z, r, t = lax.axis_index("fs"), lax.axis_index("rep"), lax.axis_index("tp")
    me = z * R + r
    every = me * T + t
    DH = m_ref.shape[1]
    FR = f_ref.shape[0]
    MR = m1_ref.shape[0]
    H, TH, FH = DH // 2, DH // TILE // 2, FR // 2
    xn, yn, dn = r + 1 - 2 * lax.rem(r, 2), lax.rem(r + 2, R), R - 1 - r

    def device(zz, rr, tt):
        return {"fs": zz, "rep": rr, "tp": tt}

    def peer(p):
        q = lax.rem(me + p, N)
        return q, q // R, lax.rem(q, R)

    def column(zz, rr):
        return pl.ds(pl.multiple_of((rr * Z + zz) * LANES, LANES), LANES)

    def rows(q, size):
        return pl.ds(pl.multiple_of(q * size, size), size)

    barrier = pltpu.get_barrier_semaphore()

    def greet(p, carry):
        q = lax.rem(every + p, N * T)
        d = q // T
        pl.semaphore_signal(
            barrier, inc=1, device_id=device(d // R, lax.rem(d, R), lax.rem(q, T)), device_id_type=MESH
        )
        return carry

    lax.fori_loop(1, N * T, greet, 0)

    def turn(i, carry):
        part = pl.ds(pl.multiple_of(i * TILE, TILE), TILE)
        mt[part, :] = m_ref[:, part].T
        return carry

    lax.fori_loop(0, DH // TILE, turn, 0)
    pl.semaphore_wait(barrier, N * T - 1)

    def product(zz, rr, store, lo=0, hi=None):
        cols = column(zz, rr)

        def tile(i, carry):
            part = pl.ds(pl.multiple_of(i * TILE, TILE), TILE)
            store(part, jnp.dot(mt[part, :], o_ref[:, cols], preferred_element_type=jnp.float32))
            return carry

        lax.fori_loop(lo, DH // TILE if hi is None else hi, tile, 0)

    def first(rr, zz, src):
        return pltpu.make_async_remote_copy(
            src_ref=send1.at[rr, zz], dst_ref=recv1.at[src, zz],
            send_sem=s1_send.at[rr, zz], recv_sem=s1_recv.at[src, zz],
            device_id=device(z, rr, t), device_id_type=MESH,
        )

    def second(zz, src):
        return pltpu.make_async_remote_copy(
            src_ref=send2.at[zz], dst_ref=recv2.at[src],
            send_sem=s2_send.at[zz], recv_sem=s2_recv.at[src],
            device_id=device(zz, r, t), device_id_type=MESH,
        )

    def via(h, zz):
        return pltpu.make_async_remote_copy(
            src_ref=send1.at[dn, zz, pl.ds(h * H, H), :], dst_ref=recvd.at[h, zz],
            send_sem=d_send.at[h, zz], recv_sem=d_recv.at[h, zz],
            device_id=device(z, yn if h else xn, t), device_id_type=MESH,
        )

    def across(e, carry):
        zz = lax.rem(z + 1 + e, Z)

        def store(part, value):
            send1[dn, zz, part, :] = value.astype(jnp.bfloat16)

        product(zz, dn, store)
        via(0, zz).start()
        via(1, zz).start()
        return carry

    lax.fori_loop(0, Z, across, 0)

    def beside(e, carry):
        zz = lax.rem(z + 1 + e, Z)
        for h, rr in ((1, xn), (0, yn)):

            def store(part, value):
                send1[rr, zz, part, :] = value.astype(jnp.bfloat16)

            def store_sum(part, value):
                inner = pl.ds(pl.multiple_of(part.start - h * H, TILE), TILE)
                total = value + recvd[h, zz, inner, :].astype(jnp.float32)
                send1[rr, zz, part, :] = total.astype(jnp.bfloat16)

            product(zz, rr, store, (1 - h) * TH, (2 - h) * TH)
            via(h, zz).wait_recv()
            product(zz, rr, store_sum, h * TH, (h + 1) * TH)
            first(rr, zz, r).start()
        return carry

    lax.fori_loop(0, Z, beside, 0)

    def f_copy(q, zz, rr, slot):
        return pltpu.make_async_remote_copy(
            src_ref=f_ref, dst_ref=f_all.at[rows(slot, FR), :],
            send_sem=fa_send.at[q], recv_sem=fa_recv.at[slot],
            device_id=device(zz, rr, t), device_id_type=MESH,
        )

    def m_copy(src, dst, ss, rs, q, zz, rr, slot):
        return pltpu.make_async_remote_copy(
            src_ref=src.at[:, column(zz, rr)], dst_ref=dst.at[rows(slot, MR), :],
            send_sem=ss.at[q], recv_sem=rs.at[slot],
            device_id=device(zz, rr, t), device_id_type=MESH,
        )

    def spread(p, carry):
        q, zz, rr = peer(p)
        f_copy(q, zz, rr, me).start()
        m_copy(m1_ref, m1_all, ma_send, ma_recv, q, zz, rr, me).start()
        m_copy(m2_ref, m2_all, mb_send, mb_recv, q, zz, rr, me).start()
        return carry

    lax.fori_loop(1, N, spread, 0)
    f_all[rows(me, FR), :] = f_ref[...]
    m1_all[rows(me, MR), :] = m1_ref[:, column(z, r)]
    m2_all[rows(me, MR), :] = m2_ref[:, column(z, r)]

    def own_block(i, carry):
        def store(part, value):
            own[i, part, :] = value

        product(i, r, store)
        return carry

    lax.fori_loop(0, Z, own_block, 0)

    def join(zz, store):
        for src in (xn, yn):
            first(src, zz, src).wait_recv()

        def tile(i, carry):
            part = pl.ds(pl.multiple_of(i * TILE, TILE), TILE)
            total = own[zz, part, :]
            for src in (xn, yn):
                total = total + recv1[src, zz, part, :].astype(jnp.float32)
            store(part, total)
            return carry

        lax.fori_loop(0, DH // TILE, tile, 0)

    def phase2(e, carry):
        zz = lax.rem(z + e, Z)

        def store(part, value):
            send2[zz, part, :] = value.astype(jnp.bfloat16)

        join(zz, store)
        second(zz, z).start()
        return carry

    lax.fori_loop(1, Z, phase2, 0)

    def store_own(part, value):
        grad[part, :] = value

    join(z, store_own)

    def wait_spread(p, carry):
        q, zz, rr = peer(p)
        f_copy(q, zz, rr, q).wait()
        m_copy(m1_ref, m1_all, ma_send, ma_recv, q, zz, rr, q).wait()
        m_copy(m2_ref, m2_all, mb_send, mb_recv, q, zz, rr, q).wait()
        return carry

    lax.fori_loop(1, N, wait_spread, 0)

    def wait_second(e, carry):
        src = lax.rem(z + e, Z)
        second(src, src).wait_recv()
        return carry

    lax.fori_loop(1, Z, wait_second, 0)

    def add_second(i, carry):
        part = pl.ds(pl.multiple_of(i * TILE, TILE), TILE)
        total = grad[part, :]
        for e in range(1, Z):
            total = total + recv2[lax.rem(z + e, Z), part, :].astype(jnp.float32)
        grad[part, :] = total
        return carry

    lax.fori_loop(0, DH // TILE, add_second, 0)

    projected = contract_rows(f_all[...], grad[...].astype(jnp.bfloat16))
    new_first = 0.8 * m1_all[...] + 0.2 * projected
    new_second = 0.9 * m2_all[...] + 0.1 * projected * projected
    nf_col[...] = new_first
    ns_col[...] = new_second
    dir_low = (new_first / (jnp.sqrt(new_second) + 1e-08)).astype(jnp.bfloat16)
    proj_low = projected.astype(jnp.bfloat16)
    dir_wide = dir_low.astype(jnp.float32)
    proj_wide = proj_low.astype(jnp.float32)
    stat[0] = jnp.broadcast_to(jnp.sum(dir_wide * dir_wide, axis=0, keepdims=True), (8, LANES))
    stat[1] = jnp.broadcast_to(jnp.sum(proj_wide * proj_wide, axis=0, keepdims=True), (8, LANES))
    stat_all[every] = stat[...]

    def s_copy(p, slot_of):
        q = lax.rem(every + p, N * T)
        d = q // T
        slot = slot_of(q)
        return pltpu.make_async_remote_copy(
            src_ref=stat, dst_ref=stat_all.at[slot],
            send_sem=st_send.at[q], recv_sem=st_recv.at[slot],
            device_id=device(d // R, lax.rem(d, R), lax.rem(q, T)), device_id_type=MESH,
        )

    def send_stat(p, carry):
        s_copy(p, lambda q: every).start()
        return carry

    lax.fori_loop(1, N * T, send_stat, 0)

    def back_copy(src, dst, size, ss, rs, q, zz, rr, sz, sr, slot):
        return pltpu.make_async_remote_copy(
            src_ref=src.at[rows(q, size), :], dst_ref=dst.at[:, column(sz, sr)],
            send_sem=ss.at[q], recv_sem=rs.at[slot],
            device_id=device(zz, rr, t), device_id_type=MESH,
        )

    def send_moments(p, carry):
        q, zz, rr = peer(p)
        back_copy(nf_col, nf_ref, MR, nf_send, nf_recv, q, zz, rr, z, r, me).start()
        back_copy(ns_col, ns_ref, MR, ns_send, ns_recv, q, zz, rr, z, r, me).start()
        return carry

    lax.fori_loop(1, N, send_moments, 0)
    nf_ref[:, column(z, r)] = nf_col[rows(me, MR), :]
    ns_ref[:, column(z, r)] = ns_col[rows(me, MR), :]

    upd_col[...] = jnp.dot(f_all[...], dir_low, preferred_element_type=jnp.float32)
    grad[...] = grad[...] - jnp.dot(f_all[...], proj_low, preferred_element_type=jnp.float32)

    def wait_stat(p, carry):
        s_copy(p, lambda q: q).wait()
        return carry

    lax.fori_loop(1, N * T, wait_stat, 0)
    totals = jnp.sum(stat_all[...], axis=0)
    dir_sum = jnp.sum(totals[0, 0:1, :], axis=1, keepdims=True)
    proj_sum = jnp.sum(totals[1, 0:1, :], axis=1, keepdims=True)
    scale_ratio = jnp.sqrt(dir_sum) / jnp.sqrt(proj_sum + 1e-06)
    upd_col[...] = upd_col[...] + scale_ratio * grad[...]

    def send_update(p, carry):
        q, zz, rr = peer(p)
        back_copy(upd_col, upd_ref, FR, up_send, up_recv, q, zz, rr, z, r, me).start()
        return carry

    lax.fori_loop(1, N, send_update, 0)
    upd_ref[:, column(z, r)] = upd_col[rows(me, FR), :]

    def wait_update(p, carry):
        q, zz, rr = peer(p)
        back_copy(upd_col, upd_ref, FR, up_send, up_recv, q, zz, rr, zz, rr, q).wait()
        return carry

    lax.fori_loop(1, N, wait_update, 0)

    new_weight = w_ref[...] - 0.01 * upd_ref[...]
    nw_ref[...] = new_weight
    wc_ref[rows(me, FR), :] = new_weight.astype(jnp.bfloat16)

    def along_z(zz, src):
        block = wc_ref.at[rows(src * R + r, FR), :]
        return pltpu.make_async_remote_copy(
            src_ref=block, dst_ref=block, send_sem=gz_send.at[zz], recv_sem=gz_recv.at[src],
            device_id=device(zz, r, t), device_id_type=MESH,
        )

    def along_r(rr, zz, src):
        block = wc_ref.at[rows(zz * R + src, FR), :]
        return pltpu.make_async_remote_copy(
            src_ref=block, dst_ref=block, send_sem=gr_send.at[rr, zz], recv_sem=gr_recv.at[src, zz],
            device_id=device(z, rr, t), device_id_type=MESH,
        )

    def start_z(e, carry):
        along_z(lax.rem(z + e, Z), z).start()
        return carry

    lax.fori_loop(1, Z, start_z, 0)

    def half(h, zz, src):
        block = wc_ref.at[pl.ds(pl.multiple_of((zz * R + src) * FR + h * FH, FH), FH), :]
        return pltpu.make_async_remote_copy(
            src_ref=block, dst_ref=block, send_sem=gh_send.at[h, zz], recv_sem=gh_recv.at[h, zz],
            device_id=device(z, xn if h else yn, t), device_id_type=MESH,
        )

    def relay(e, carry):
        zz = lax.rem(z + 2 * Z - e, Z)
        last = lax.rem(z + 2 * Z - e + 1, Z)

        @pl.when(e < Z)
        def _():
            @pl.when(e > 0)
            def _():
                along_z(zz, zz).wait_recv()

            along_r(xn, zz, r).start()
            along_r(yn, zz, r).start()

        @pl.when(e > 0)
        def _():
            along_r(xn, last, xn).wait_recv()
            half(0, last, xn).start()
            along_r(yn, last, yn).wait_recv()
            half(1, last, yn).start()

        return carry

    lax.fori_loop(0, Z + 1, relay, 0)

    def drain(zz, carry):
        for h, rr in ((0, xn), (1, yn)):
            along_r(rr, zz, r).wait_send()
            first(rr, zz, r).wait_send()
            via(h, zz).wait_send()
            half(h, zz, rr).wait_send()
            half(h, zz, dn).wait_recv()
        return carry

    lax.fori_loop(0, Z, drain, 0)

    def drain_z(e, carry):
        zz = lax.rem(z + e, Z)
        along_z(zz, z).wait_send()
        second(zz, z).wait_send()
        return carry

    lax.fori_loop(1, Z, drain_z, 0)

    def drain_moments(p, carry):
        q, zz, rr = peer(p)
        back_copy(nf_col, nf_ref, MR, nf_send, nf_recv, q, zz, rr, zz, rr, q).wait()
        back_copy(ns_col, ns_ref, MR, ns_send, ns_recv, q, zz, rr, zz, rr, q).wait()
        return carry

    lax.fori_loop(1, N, drain_moments, 0)


def fused(Z, R, T, *args):
    mixer_out, out_grad, factors, weight, first_moment, second_moment = args
    N = Z * R
    DH = mixer_out.shape[1]
    rank = factors.shape[1]
    f32, bf16 = jnp.float32, jnp.bfloat16
    vmem = pl.BlockSpec(memory_space=pltpu.VMEM)
    dma = pltpu.SemaphoreType.DMA
    wide = lambda n: [dma((n,)), dma((n,))]
    return pl.pallas_call(
        functools.partial(fused_kernel, Z, R, T),
        out_shape=(
            jax.ShapeDtypeStruct(weight.shape, f32),
            jax.ShapeDtypeStruct(weight.shape, f32),
            jax.ShapeDtypeStruct(first_moment.shape, f32),
            jax.ShapeDtypeStruct(first_moment.shape, f32),
            jax.ShapeDtypeStruct((DH, weight.shape[1]), bf16),
        ),
        in_specs=[vmem] * 6,
        out_specs=(vmem,) * 5,
        scratch_shapes=[
            pltpu.VMEM((DH, mixer_out.shape[0]), bf16),
            pltpu.VMEM((R, Z, DH, LANES), bf16),
            pltpu.VMEM((R, Z, DH, LANES), bf16),
            pltpu.VMEM((Z, DH, LANES), f32),
            pltpu.VMEM((Z, DH, LANES), bf16),
            pltpu.VMEM((Z, DH, LANES), bf16),
            pltpu.VMEM((DH, LANES), f32),
            pltpu.VMEM((DH, rank), bf16),
            pltpu.VMEM((rank, LANES), f32),
            pltpu.VMEM((rank, LANES), f32),
            pltpu.VMEM((rank, LANES), f32),
            pltpu.VMEM((rank, LANES), f32),
            pltpu.VMEM((DH, LANES), f32),
            pltpu.VMEM((2, 8, LANES), f32),
            pltpu.VMEM((N * T, 2, 8, LANES), f32),
            dma((R, Z)), dma((R, Z)), *wide(Z),
            *wide(N), *wide(N), *wide(N),
            *wide(N * T), *wide(N), *wide(N), *wide(N),
            *wide(Z), dma((R, Z)), dma((R, Z)),
            pltpu.VMEM((2, Z, DH // 2, LANES), bf16),
            dma((2, Z)), dma((2, Z)), dma((2, Z)), dma((2, Z)),
        ],
        compiler_params=pltpu.CompilerParams(
            collective_id=0, has_side_effects=True, vmem_limit_bytes=60 * 1024 * 1024
        ),
    )(*args)

def plain(mixer_out, out_grad, factors, weight, first_moment, second_moment):
    columns = mixer_out
    gradient = lax.psum_scatter(
        contract_rows(columns, out_grad), ("fs", "rep"), scatter_dimension=0, tiled=True
    )
    grad_low = gradient.astype(jnp.bfloat16)
    columns = factors
    projected = lax.psum_scatter(
        contract_rows(columns, grad_low), ("fs", "rep"), scatter_dimension=0, tiled=True
    )
    new_first = 0.8 * first_moment + 0.2 * projected
    new_second = 0.9 * second_moment + 0.1 * projected * projected
    direction = new_first / (jnp.sqrt(new_second) + 1e-08)
    dir_low = direction.astype(jnp.bfloat16)
    proj_low = projected.astype(jnp.bfloat16)
    dir_whole, proj_whole = (
        lax.all_gather(dir_low, ("fs", "rep"), axis=0, tiled=True),
        lax.all_gather(proj_low, ("fs", "rep"), axis=0, tiled=True),
    )
    dir_wide = dir_low.astype(jnp.float32)
    proj_wide = proj_low.astype(jnp.float32)
    dir_sum, proj_sum = lax.psum(
        (jnp.sum(dir_wide * dir_wide), jnp.sum(proj_wide * proj_wide)), ("fs", "rep", "tp")
    )
    back_dir = jnp.dot(factors, dir_whole, preferred_element_type=jnp.float32)
    back_proj = jnp.dot(factors, proj_whole, preferred_element_type=jnp.float32)
    scale_ratio = jnp.sqrt(dir_sum) / jnp.sqrt(proj_sum + 1e-06)
    update = back_dir + scale_ratio * (gradient - back_proj)
    new_weight = weight - 0.01 * update
    weight_copy = lax.all_gather(new_weight.astype(jnp.bfloat16), ("fs", "rep"), axis=0, tiled=True)
    return (new_weight, update, new_first, new_second, weight_copy)


def solution(mesh):
    Z, R, T = mesh.shape["fs"], mesh.shape["rep"], mesh.shape["tp"]

    def per_device(*args):
        mixer_out, out_grad, factors, weight, first_moment, second_moment = args
        fits = (
            out_grad.shape[1] == Z * R * LANES
            and mixer_out.shape[1] % (2 * TILE) == 0
            and weight.shape[0] % 32 == 0
            and first_moment.shape[0] % 8 == 0
            and R == 4
            and Z > 1
        )
        return fused(Z, R, T, *args) if fits else plain(*args)

    in_specs = (
        P(("fs", "rep"), None),
        P(("fs", "rep"), "tp"),
        P(("fs", "rep"), None),
        P(("fs", "rep"), "tp"),
        P(("fs", "rep"), "tp"),
        P(("fs", "rep"), "tp"),
    )
    out_specs = (
        P(("fs", "rep"), "tp"),
        P(("fs", "rep"), "tp"),
        P(("fs", "rep"), "tp"),
        P(("fs", "rep"), "tp"),
        P(None, "tp"),
    )
    return jax.shard_map(
        per_device, mesh=mesh, in_specs=in_specs, out_specs=out_specs, check_vma=False
    )
```

profile of v0, /device:TPU:18, one launch (start us, length us, event | category | flops | bytes accessed | tf_op | source)
XLA Modules:
  0.0 214.6 jit_solution(9630032758656842657)
XLA Ops:
  0.6 200.1 %shard_map.101 = (f32[96,2048]{1,0:T(8,128)}, f32[96,2048]{1,0:T(8,128)}, f32[16,2048]{1,0:T(8,128)}, f32[16,2048]{1,0:T(8,128)}, bf16[1536,2048]{1,0:T(8,128)(2,1)}) custom-call(bf16[1024,1536]{1,0:T(8,128)(2,1)} %m_ref.1, bf16[1024,2048]{1,0:T(8,128)(2,1)} %o_ref.1, bf16[96,256]{1,0:T(8,128)(2,1)} %f_ref.1, f32[96,2048]{1,0:T(8,128)} %w_ref.1, ...), custom_call_target="tpu_custom_call" | custom-call | tf_op jit(solution)/shard_map/pallas_call | solution.py:399
  200.7 2.1 copy.16
  202.8 2.1 copy.17
  204.8 1.6 copy.18
  206.4 1.6 copy.19
  208.0 6.6 %copy.20 = bf16[1536,2048]{1,0:T(8,128)(2,1)} copy(bf16[1536,2048]{1,0:T(8,128)(2,1)} %get-tuple-element.14) | data formatting | bytes 12582912
where the time goes:
time: 215 us
  Pallas kernels  200 us (93%)
  local copies, waits for them, and re-layouts  13.9 us (6%)
    pallas_call x1, Pallas kernels, fused(): pl.pallas_call(functools.partial(fused_kernel, Z, R, T), out_shape=(jax.S...  200 us
    unnamed x5, local copies, waits for them, and re-layouts  13.9 us

commit v1 on v0

--- a/solution.py
+++ b/solution.py
@@ -387,6 +387,27 @@
     lax.fori_loop(1, N, drain_moments, 0)
 
 
+def drain_kernel(*refs):
+    n = len(refs) // 2
+    ins, outs, sem = refs[:n], refs[n:-1], refs[-1]
+    copies = [pltpu.make_async_copy(a, b, sem.at[i]) for i, (a, b) in enumerate(zip(ins, outs))]
+    for c in copies:
+        c.start()
+    for c in copies:
+        c.wait()
+
+
+def drain_out(*arrays):
+    return pl.pallas_call(
+        drain_kernel,
+        out_shape=tuple(jax.ShapeDtypeStruct(a.shape, a.dtype) for a in arrays),
+        in_specs=[pl.BlockSpec(memory_space=pltpu.VMEM)] * len(arrays),
+        out_specs=(pl.BlockSpec(memory_space=pl.ANY),) * len(arrays),
+        scratch_shapes=[pltpu.SemaphoreType.DMA((len(arrays),))],
+        compiler_params=pltpu.CompilerParams(vmem_limit_bytes=4 * 1024 * 1024),
+    )(*[pltpu.with_memory_space_constraint(a, pltpu.VMEM) for a in arrays])
+
+
 def fused(Z, R, T, *args):
     mixer_out, out_grad, factors, weight, first_moment, second_moment = args
     N = Z * R
@@ -396,14 +417,14 @@
     vmem = pl.BlockSpec(memory_space=pltpu.VMEM)
     dma = pltpu.SemaphoreType.DMA
     wide = lambda n: [dma((n,)), dma((n,))]
-    return pl.pallas_call(
+    return drain_out(*pl.pallas_call(
         functools.partial(fused_kernel, Z, R, T),
         out_shape=(
-            jax.ShapeDtypeStruct(weight.shape, f32),
-            jax.ShapeDtypeStruct(weight.shape, f32),
-            jax.ShapeDtypeStruct(first_moment.shape, f32),
-            jax.ShapeDtypeStruct(first_moment.shape, f32),
-            jax.ShapeDtypeStruct((DH, weight.shape[1]), bf16),
+            pltpu.VMEM(weight.shape, f32),
+            pltpu.VMEM(weight.shape, f32),
+            pltpu.VMEM(first_moment.shape, f32),
+            pltpu.VMEM(first_moment.shape, f32),
+            pltpu.VMEM((DH, weight.shape[1]), bf16),
         ),
         in_specs=[vmem] * 6,
         out_specs=(vmem,) * 5,
@@ -431,9 +452,9 @@
             dma((2, Z)), dma((2, Z)), dma((2, Z)), dma((2, Z)),
         ],
         compiler_params=pltpu.CompilerParams(
-            collective_id=0, has_side_effects=True, vmem_limit_bytes=60 * 1024 * 1024
+            collective_id=0, has_side_effects=True, vmem_limit_bytes=48 * 1024 * 1024
         ),
-    )(*args)
+    )(*args))
 
 def plain(mixer_out, out_grad, factors, weight, first_moment, second_moment):
     columns = mixer_out

time: 215 us -> 201 us (0.935)
  local copies, waits for them, and re-layouts: 13.9 us -> 0 us
    unnamed x5 -> x0, local copies, waits for them, and re-layouts: 13.9 us -> none
    pallas_call x1 -> x2, Pallas kernels: 200 us -> 200 us  [the longest x1 197 us: fused(): pl.pallas_call(functools.partial(fused_kernel, Z, R, T), out_shape=(pltpu...]
where the time goes in v1:
time: 201 us
  Pallas kernels  200 us (100%)
    pallas_call x1, Pallas kernels, fused(): pl.pallas_call(functools.partial(fused_kernel, Z, R, T), out_shape=(pltpu...  197 us

profile of v1, /device:TPU:18, one launch (start us, length us, event | category | flops | bytes accessed | tf_op | source)
XLA Modules:
  0.0 200.7 jit_solution(1592354273091868206)
XLA Ops:
  0.6 196.7 %shard_map.101 = (f32[96,2048]{1,0:T(8,128)S(1)}, f32[96,2048]{1,0:T(8,128)S(1)}, f32[16,2048]{1,0:T(8,128)S(1)}, f32[16,2048]{1,0:T(8,128)S(1)}, bf16[1536,2048]{1,0:T(8,128)(2,1)S(1)}) custom-call(bf16[1024,1536]{1,0:T(8,128)(2,1)} %m_ref.1, bf16[1024,2048]{1,0:T(8,128)(2,1)} %o_ref.1, bf16[96,256]{1,0:T(8,128)(2,1)} %f_ref.1, f32[96,2048]{1,0:T(8,128)} %w_ref.1, ...), custom_call_target="tpu_custom_call" | custom-call | tf_op jit(solution)/shard_map/pallas_call | solution.py:420
  197.4 3.4 %shard_map.102 = (f32[96,2048]{1,0:T(8,128)}, f32[96,2048]{1,0:T(8,128)}, f32[16,2048]{1,0:T(8,128)}, f32[16,2048]{1,0:T(8,128)}, bf16[1536,2048]{1,0:T(8,128)(2,1)}) custom-call(f32[96,2048]{1,0:T(8,128)S(1)} %get-tuple-element.10.refs_0_, f32[96,2048]{1,0:T(8,128)S(1)} %get-tuple-element.11.refs_1_, f32[16,2048]{1,0:T(8,128)S(1)} %get-tuple-element.12.refs_2_, ...), custom_call_target="tpu_custom_call" | custom-call | tf_op jit(solution)/shard_map/pallas_call | solution.py:401

commit v2 on v0

v2 whole, which is shorter than its diff:
```python
import functools

import jax
import jax.numpy as jnp
from jax import lax
from jax.experimental import pallas as pl
from jax.experimental.pallas import tpu as pltpu
from jax.sharding import PartitionSpec as P

MESH = pl.DeviceIdType.MESH
LANES = 128
PAIR = 2 * LANES
RING = 4
START_GATHER = 10
VMEM_GRANT = 52 * 1024 * 1024


def contract_rows(left, right):
    return lax.dot_general(
        left, right, (((0,), (0,)), ((), ())), preferred_element_type=jnp.float32
    )


def drain_kernel(*refs):
    n = len(refs) // 2
    ins, outs, sem = refs[:n], refs[n:-1], refs[-1]
    copies = [pltpu.make_async_copy(a, b, sem.at[i]) for i, (a, b) in enumerate(zip(ins, outs))]
    for c in copies:
        c.start()
    for c in copies:
        c.wait()


def drain_out(*arrays):
    return pl.pallas_call(
        drain_kernel,
        out_shape=tuple(jax.ShapeDtypeStruct(a.shape, a.dtype) for a in arrays),
        in_specs=[pl.BlockSpec(memory_space=pltpu.VMEM)] * len(arrays),
        out_specs=(pl.BlockSpec(memory_space=pl.ANY),) * len(arrays),
        scratch_shapes=[pltpu.SemaphoreType.DMA((len(arrays),))],
        compiler_params=pltpu.CompilerParams(vmem_limit_bytes=4 * 1024 * 1024),
    )(*[pltpu.with_memory_space_constraint(a, pltpu.VMEM) for a in arrays])


def fused_kernel(
    Z, R, T,
    m_ref, o_ref, f_ref, w_ref, m1_ref, m2_ref,
    nw_ref, upd_ref, nf_ref, ns_ref, wc_ref,
    mt, own, s1, r1, s2, r2, s3, r3,
    f_all, ft, yt, own_p, s1_p, r1_p, s2_p, r2_p, s3_p, r3_p, proj, q_all, q_own,
    stat, stat_all, ratio,
    t_send, t_recv, u_send, u_recv, v_send, v_recv,
    tp_send, tp_recv, up_send, up_recv, vp_send, vp_recv,
    gz_send, gz_recv, gx_send, gx_recv,
    st_send, st_recv,
):
    N = Z * R
    z, r, t = lax.axis_index("fs"), lax.axis_index("rep"), lax.axis_index("tp")
    every = (z * R + r) * T + t
    TOK, DH = m_ref.shape
    CW = o_ref.shape[1]
    FR, RK = f_ref.shape
    MR = m1_ref.shape[0]
    NP = CW // PAIR
    K = START_GATHER
    HALF = CW // 2
    xn, yn, dn = r + 1 - 2 * lax.rem(r, 2), lax.rem(r + 2, R), R - 1 - r
    near = ((xn, yn), (yn, xn))
    f32, bf16 = jnp.float32, jnp.bfloat16

    def device(zz, rr, tt):
        return {"fs": zz, "rep": rr, "tp": tt}

    def lanes(index, size):
        return pl.ds(pl.multiple_of(index * size, size), size)

    def other(e):
        return lax.rem(z + e, Z)

    def each_z(body):
        def step(e, carry):
            body(other(e))
            return carry

        lax.fori_loop(1, Z, step, 0)

    barrier = pltpu.get_barrier_semaphore()

    def greet(p, carry):
        q = lax.rem(every + p, N * T)
        d = q // T
        pl.semaphore_signal(
            barrier, inc=1, device_id=device(d // R, lax.rem(d, R), lax.rem(q, T)), device_id_type=MESH
        )
        return carry

    lax.fori_loop(1, N * T, greet, 0)

    def turn(i, carry):
        mt[lanes(i, PAIR), :] = m_ref[:, lanes(i, PAIR)].T
        return carry

    lax.fori_loop(0, DH // PAIR, turn, 0)

    def move(src, dst, ss, rs, where):
        return pltpu.make_async_remote_copy(
            src_ref=src, dst_ref=dst, send_sem=ss, recv_sem=rs, device_id=where, device_id_type=MESH
        )

    class Scatter:
        def __init__(self, c, h, slot, refs, sems):
            self.c, self.h, self.slot = c, h, slot
            self.own, self.s1, self.r1, self.s2, self.r2, self.s3, self.r3 = refs
            self.ts, self.tr, self.us, self.ur, self.vs, self.vr = sems
            self.n1, self.n2 = near[h]

        def first(self, k):
            rr = self.n1 if k else dn
            c = self.c
            return move(self.s1.at[c, rr], self.r1.at[c, k], self.ts.at[c, k], self.tr.at[c, k], device(z, self.n1, t))

        def second(self):
            c = self.c
            return move(self.s2.at[c], self.r2.at[c], self.us.at[c], self.ur.at[c], device(z, self.n2, t))

        def third(self, zz, src):
            c = self.c
            return move(
                self.s3.at[c, zz], self.r3.at[c, src], self.vs.at[c, zz], self.vr.at[c, src], device(zz, r, t)
            )

        def mine(self, rr, zz):
            return self.own[self.slot, self.h, rr, zz]

        def stage2(self):
            c = self.c
            self.first(0).wait_recv()

            def add(zz, carry):
                total = self.mine(self.n2, zz) + self.r1[c, 0, zz].astype(f32)
                self.s2[c, zz] = total.astype(bf16)
                return carry

            lax.fori_loop(0, Z, add, 0)
            self.second().start()

        def stage3(self, put):
            c = self.c
            self.first(1).wait_recv()
            self.second().wait_recv()

            def total(zz):
                return self.mine(r, zz) + self.r1[c, 1, zz].astype(f32) + self.r2[c, zz].astype(f32)

            def send(zz):
                self.s3[c, zz] = total(zz).astype(bf16)
                self.third(zz, z).start()

            each_z(send)
            put(total(z))

        def last(self, get, put):
            each_z(lambda zz: self.third(zz, zz).wait_recv())
            value = get()
            for e in range(1, Z):
                value = value + self.r3[self.c, other(e)].astype(f32)
            put(value)

        def sent(self):
            self.first(0).wait_send()
            self.first(1).wait_send()
            self.second().wait_send()
            each_z(lambda zz: self.third(zz, z).wait_send())

    class Gather:
        def __init__(self, g, h, ref, cols):
            self.g, self.ref, self.cols = g, ref, cols
            self.n1, self.n2 = near[h]

        def along(self, zz, src_z, block=None):
            place = self.ref.at[src_z, r, :, self.cols]
            return move(
                place if block is None else block, place,
                gz_send.at[self.g, zz], gz_recv.at[self.g, src_z], device(zz, r, t),
            )

        def beside(self, k, rr):
            place = self.ref.at[:, rr, :, self.cols]
            to = self.n2 if k == 0 else self.n1
            return move(place, place, gx_send.at[self.g, k], gx_recv.at[self.g, k], device(z, to, t))

        def stage1(self, block=None):
            each_z(lambda zz: self.along(zz, z, block).start())

        def stage2(self):
            each_z(lambda zz: self.along(zz, zz).wait_recv())
            self.beside(0, r).start()
            self.beside(1, r).start()

        def stage3(self):
            self.beside(0, self.n2).wait_recv()
            self.beside(2, self.n2).start()

        def done(self):
            self.beside(1, self.n1).wait_recv()
            self.beside(2, dn).wait_recv()
            each_z(lambda zz: self.along(zz, z).wait_send())
            self.beside(0, r).wait_send()
            self.beside(1, r).wait_send()
            self.beside(2, self.n2).wait_send()

    main_refs = (own, s1, r1, s2, r2, s3, r3)
    main_sems = (t_send, t_recv, u_send, u_recv, v_send, v_recv)
    proj_refs = (own_p, s1_p, r1_p, s2_p, r2_p, s3_p, r3_p)
    proj_sems = (tp_send, tp_recv, up_send, up_recv, vp_send, vp_recv)

    def scatter(p, h):
        return Scatter(2 * p + h, h, lax.rem(p, RING), main_refs, main_sems)

    def scatter_p(h):
        return Scatter(h, h, 0, proj_refs, proj_sems)

    def gather_w(p, h):
        return Gather(2 * p + h, h, wc_ref, lanes(2 * p + h, LANES))

    def gather_f(h):
        return Gather(2 * NP + h, h, f_all, pl.ds(h * (RK // 2), RK // 2))

    def gather_q(h):
        return Gather(2 * NP + 2 + h, h, q_all, pl.ds(h * HALF, HALF))

    f_all[z, r] = f_ref[...]
    pl.semaphore_wait(barrier, N * T - 1)
    for h in (0, 1):
        gather_f(h).stage1(f_ref.at[:, pl.ds(h * (RK // 2), RK // 2)])

    def product(p):
        cols = lanes(p, PAIR)
        slot = lax.rem(p, RING)
        G = R * FR

        def tile(zz, carry):
            part = pl.ds(pl.multiple_of(zz * G, G), G)
            value = jnp.dot(mt[part, :], o_ref[:, cols], preferred_element_type=f32)
            for h in (0, 1):
                for rr in range(R):
                    block = value[rr * FR : (rr + 1) * FR, h * LANES : (h + 1) * LANES]
                    own[slot, h, rr, zz] = block
                    s1[2 * p + h, rr, zz] = block.astype(bf16)
            return carry

        lax.fori_loop(0, Z, tile, 0)
        for k in (0, 1):
            for h in (0, 1):
                scatter(p, h).first(k).start()

    def project():
        ft[...] = f_all[...].reshape(DH, RK).T

        def low(i, carry):
            yt[:, lanes(i, PAIR)] = jnp.dot(
                ft[...], mt[:, lanes(i, PAIR)], preferred_element_type=f32
            ).astype(bf16)
            return carry

        lax.fori_loop(0, TOK // PAIR, low, 0)

        def tile(n, carry):
            value = jnp.dot(yt[...], o_ref[:, lanes(n, PAIR)], preferred_element_type=f32)
            h = n // (NP // 2)
            cols = lanes(lax.rem(n, NP // 2), PAIR)
            for zz in range(Z):
                for rr in range(R):
                    low_row = (zz * R + rr) * MR
                    block = value[low_row : low_row + MR, :]
                    own_p[0, h, rr, zz, :, cols] = block
                    s1_p[h, rr, zz, :, cols] = block.astype(bf16)
            return carry

        lax.fori_loop(0, NP, tile, 0)

    def s_copy(p, slot_of):
        q = lax.rem(every + p, N * T)
        d = q // T
        slot = slot_of(q)
        return move(
            stat, stat_all.at[slot], st_send.at[q], st_recv.at[slot],
            device(d // R, lax.rem(d, R), lax.rem(q, T)),
        )

    def fold(value):
        row = jnp.sum(value, axis=0, keepdims=True)
        total = row[:, :LANES]
        for j in range(1, CW // LANES):
            total = total + row[:, j * LANES : (j + 1) * LANES]
        return jnp.broadcast_to(total, (8, LANES))

    def moments():
        projected = proj[...]
        new_first = 0.8 * m1_ref[...] + 0.2 * projected
        new_second = 0.9 * m2_ref[...] + 0.1 * projected * projected
        nf_ref[...] = new_first
        ns_ref[...] = new_second
        dir_wide = (new_first / (jnp.sqrt(new_second) + 1e-08)).astype(bf16).astype(f32)
        proj_wide = projected.astype(bf16).astype(f32)
        stat[0] = fold(dir_wide * dir_wide)
        stat[1] = fold(proj_wide * proj_wide)
        stat_all[every] = stat[...]

        def send(p, carry):
            s_copy(p, lambda q: every).start()
            return carry

        lax.fori_loop(1, N * T, send, 0)

    def combine():
        def wait(p, carry):
            s_copy(p, lambda q: q).wait()
            return carry

        lax.fori_loop(1, N * T, wait, 0)
        totals = jnp.sum(stat_all[...], axis=0)
        dir_sum = jnp.sum(totals[0, 0:1, :], axis=1, keepdims=True)
        proj_sum = jnp.sum(totals[1, 0:1, :], axis=1, keepdims=True)
        scale_ratio = jnp.sqrt(dir_sum) / jnp.sqrt(proj_sum + 1e-06)
        ratio[...] = jnp.broadcast_to(scale_ratio, (8, PAIR))
        projected = proj[...]
        dir_wide = (nf_ref[...] / (jnp.sqrt(ns_ref[...]) + 1e-08)).astype(bf16).astype(f32)
        mixed = (dir_wide - scale_ratio * projected.astype(bf16).astype(f32)).astype(bf16)
        q_own[...] = mixed
        q_all[z, r] = mixed
        for h in (0, 1):
            gather_q(h).stage1(q_own.at[:, pl.ds(h * HALF, HALF)])

    def put_proj(h):
        def put(value):
            proj[:, h * HALF : (h + 1) * HALF] = value

        return put

    def get_proj(h):
        return lambda: proj[:, h * HALF : (h + 1) * HALF]

    def both(action):
        for h in (0, 1):
            action(h)

    def event_project():
        both(lambda h: gather_f(h).done())
        project()
        for k in (0, 1):
            both(lambda h: scatter_p(h).first(k).start())

    def event_moments():
        both(lambda h: scatter_p(h).last(get_proj(h), put_proj(h)))
        moments()

    events = {
        1: lambda: both(lambda h: gather_f(h).stage2()),
        2: lambda: both(lambda h: gather_f(h).stage3()),
        3: event_project,
        4: lambda: both(lambda h: scatter_p(h).stage2()),
        5: lambda: both(lambda h: scatter_p(h).stage3(put_proj(h))),
        6: event_moments,
        7: combine,
        8: lambda: both(lambda h: gather_q(h).stage2()),
        9: lambda: both(lambda h: gather_q(h).stage3()),
        10: lambda: both(lambda h: (gather_q(h).done(), scatter_p(h).sent())),
    }

    def put_grad(p, h):
        def put(value):
            upd_ref[:, lanes(2 * p + h, LANES)] = value

        return put

    def get_grad(p, h):
        return lambda: upd_ref[:, lanes(2 * p + h, LANES)]

    def update(p):
        cols = lanes(p, PAIR)
        mixed = q_all[:, :, :, cols].reshape(RK, PAIR)
        value = jnp.dot(f_ref[...], mixed, preferred_element_type=f32) + ratio[0:1, :] * upd_ref[:, cols]
        upd_ref[:, cols] = value
        new_weight = w_ref[:, cols] - 0.01 * value
        nw_ref[:, cols] = new_weight
        wc_ref[z, r, :, cols] = new_weight.astype(bf16)
        both(lambda h: gather_w(p, h).stage1())

    def tick(i, carry):
        def within(lag, action):
            @pl.when((i >= lag) & (i < lag + NP))
            def _():
                action(i - lag)

        for when, action in events.items():
            pl.when(i == when)(action)
        within(0, product)
        within(1, lambda p: both(lambda h: scatter(p, h).stage2()))
        within(2, lambda p: both(lambda h: scatter(p, h).stage3(put_grad(p, h))))
        within(3, lambda p: both(lambda h: scatter(p, h).last(get_grad(p, h), put_grad(p, h))))
        within(4, lambda p: both(lambda h: scatter(p, h).sent()))
        within(K, update)
        within(K + 1, lambda p: both(lambda h: gather_w(p, h).stage2()))
        within(K + 2, lambda p: both(lambda h: gather_w(p, h).stage3()))
        within(K + 3, lambda p: both(lambda h: gather_w(p, h).done()))
        return carry

    lax.fori_loop(0, NP + K + 3, tick, 0)


def fused(Z, R, T, *args):
    mixer_out, out_grad, factors, weight, first_moment, second_moment = args
    N = Z * R
    TOK, DH = mixer_out.shape
    FR, RK = factors.shape
    MR, CW = first_moment.shape
    NC, HALF = CW // LANES, CW // 2
    f32, bf16 = jnp.float32, jnp.bfloat16
    vmem = pl.BlockSpec(memory_space=pltpu.VMEM)
    dma = pltpu.SemaphoreType.DMA
    pair = lambda *shape: [dma(shape), dma(shape)]
    outs = pl.pallas_call(
        functools.partial(fused_kernel, Z, R, T),
        out_shape=(
            pltpu.VMEM(weight.shape, f32),
            pltpu.VMEM(weight.shape, f32),
            pltpu.VMEM(first_moment.shape, f32),
            pltpu.VMEM(first_moment.shape, f32),
            pltpu.VMEM((Z, R, FR, CW), bf16),
        ),
        in_specs=[vmem] * 6,
        out_specs=(vmem,) * 5,
        scratch_shapes=[
            pltpu.VMEM((DH, TOK), bf16),
            pltpu.VMEM((RING, 2, R, Z, FR, LANES), f32),
            pltpu.VMEM((NC, R, Z, FR, LANES), bf16),
            pltpu.VMEM((NC, 2, Z, FR, LANES), bf16),
            pltpu.VMEM((NC, Z, FR, LANES), bf16),
            pltpu.VMEM((NC, Z, FR, LANES), bf16),
            pltpu.VMEM((NC, Z, FR, LANES), bf16),
            pltpu.VMEM((NC, Z, FR, LANES), bf16),
            pltpu.VMEM((Z, R, FR, RK), bf16),
            pltpu.VMEM((RK, DH), bf16),
            pltpu.VMEM((RK, TOK), bf16),
            pltpu.VMEM((1, 2, R, Z, MR, HALF), f32),
            pltpu.VMEM((2, R, Z, MR, HALF), bf16),
            pltpu.VMEM((2, 2, Z, MR, HALF), bf16),
            pltpu.VMEM((2, Z, MR, HALF), bf16),
            pltpu.VMEM((2, Z, MR, HALF), bf16),
            pltpu.VMEM((2, Z, MR, HALF), bf16),
            pltpu.VMEM((2, Z, MR, HALF), bf16),
            pltpu.VMEM((MR, CW), f32),
            pltpu.VMEM((Z, R, MR, CW), bf16),
            pltpu.VMEM((MR, CW), bf16),
            pltpu.VMEM((2, 8, LANES), f32),
            pltpu.VMEM((N * T, 2, 8, LANES), f32),
            pltpu.VMEM((8, PAIR), f32),
            *pair(NC, 2), *pair(NC), *pair(NC, Z),
            *pair(2, 2), *pair(2), *pair(2, Z),
            *pair(NC + 4, Z), *pair(NC + 4, 3),
            *pair(N * T),
        ],
        compiler_params=pltpu.CompilerParams(
            collective_id=0, has_side_effects=True, vmem_limit_bytes=VMEM_GRANT
        ),
    )(*args)
    new_weight, update, new_first, new_second, copy = drain_out(*outs)
    return new_weight, update, new_first, new_second, copy.reshape(DH, CW)


def plain(mixer_out, out_grad, factors, weight, first_moment, second_moment):
    columns = mixer_out
    gradient = lax.psum_scatter(
        contract_rows(columns, out_grad), ("fs", "rep"), scatter_dimension=0, tiled=True
    )
    grad_low = gradient.astype(jnp.bfloat16)
    columns = factors
    projected = lax.psum_scatter(
        contract_rows(columns, grad_low), ("fs", "rep"), scatter_dimension=0, tiled=True
    )
    new_first = 0.8 * first_moment + 0.2 * projected
    new_second = 0.9 * second_moment + 0.1 * projected * projected
    direction = new_first / (jnp.sqrt(new_second) + 1e-08)
    dir_low = direction.astype(jnp.bfloat16)
    proj_low = projected.astype(jnp.bfloat16)
    dir_whole, proj_whole = (
        lax.all_gather(dir_low, ("fs", "rep"), axis=0, tiled=True),
        lax.all_gather(proj_low, ("fs", "rep"), axis=0, tiled=True),
    )
    dir_wide = dir_low.astype(jnp.float32)
    proj_wide = proj_low.astype(jnp.float32)
    dir_sum, proj_sum = lax.psum(
        (jnp.sum(dir_wide * dir_wide), jnp.sum(proj_wide * proj_wide)), ("fs", "rep", "tp")
    )
    back_dir = jnp.dot(factors, dir_whole, preferred_element_type=jnp.float32)
    back_proj = jnp.dot(factors, proj_whole, preferred_element_type=jnp.float32)
    scale_ratio = jnp.sqrt(dir_sum) / jnp.sqrt(proj_sum + 1e-06)
    update = back_dir + scale_ratio * (gradient - back_proj)
    new_weight = weight - 0.01 * update
    weight_copy = lax.all_gather(new_weight.astype(jnp.bfloat16), ("fs", "rep"), axis=0, tiled=True)
    return (new_weight, update, new_first, new_second, weight_copy)


def solution(mesh):
    Z, R, T = mesh.shape["fs"], mesh.shape["rep"], mesh.shape["tp"]

    def per_device(*args):
        mixer_out, out_grad, factors, weight, first_moment, second_moment = args
        fits = (
            out_grad.shape[1] % (4 * PAIR) == 0
            and mixer_out.shape[0] % PAIR == 0
            and mixer_out.shape[1] % PAIR == 0
            and weight.shape[0] % 16 == 0
            and first_moment.shape[0] % 16 == 0
            and factors.shape[1] == PAIR
            and R == 4
            and Z > 1
        )
        return fused(Z, R, T, *args) if fits else plain(*args)

    in_specs = (
        P(("fs", "rep"), None),
        P(("fs", "rep"), "tp"),
        P(("fs", "rep"), None),
        P(("fs", "rep"), "tp"),
        P(("fs", "rep"), "tp"),
        P(("fs", "rep"), "tp"),
    )
    out_specs = (
        P(("fs", "rep"), "tp"),
        P(("fs", "rep"), "tp"),
        P(("fs", "rep"), "tp"),
        P(("fs", "rep"), "tp"),
        P(None, "tp"),
    )
    return jax.shard_map(
        per_device, mesh=mesh, in_specs=in_specs, out_specs=out_specs, check_vma=False
    )
```

time: 215 us -> 162 us (0.75)
  the two profiles are of different devices: /device:TPU:18 before, /device:TPU:0 now
where the time goes in v2:
time: 162 us
  Pallas kernels  161 us (99%)
    pallas_call x1, Pallas kernels, fused(): pl.pallas_call(functools.partial(fused_kernel, Z, R, T), out_shape=(pltpu...  158 us
    pallas_call x1, Pallas kernels, drain_out(): pl.pallas_call(drain_kernel, out_shape=tuple((jax.ShapeDtypeStruct(a.shap...  3.35 us

profile of v2, /device:TPU:0, one launch (start us, length us, event | category | flops | bytes accessed | tf_op | source)
XLA Modules:
  0.0 162.0 jit_solution(428897040921469888)
XLA Ops:
  0.6 158.0 %shard_map.101 = (f32[96,2048]{1,0:T(8,128)S(1)}, f32[96,2048]{1,0:T(8,128)S(1)}, f32[16,2048]{1,0:T(8,128)S(1)}, f32[16,2048]{1,0:T(8,128)S(1)}, bf16[4,4,96,2048]{3,2,1,0:T(8,128)(2,1)S(1)}) custom-call(bf16[1024,1536]{1,0:T(8,128)(2,1)} %m_ref.1, bf16[1024,2048]{1,0:T(8,128)(2,1)} %o_ref.1, bf16[96,256]{1,0:T(8,128)(2,1)} %f_ref.1, f32[96,2048]{1,0:T(8,128)} %w_ref.1, ...), custom_call_target="tpu_custom_call" | custom-call | tf_op jit(solution)/shard_map/pallas_call | solution.py:423
  158.6 3.4 %shard_map.102 = (f32[96,2048]{1,0:T(8,128)}, f32[96,2048]{1,0:T(8,128)}, f32[16,2048]{1,0:T(8,128)}, f32[16,2048]{1,0:T(8,128)}, bf16[4,4,96,2048]{3,2,1,0:T(8,128)(2,1)}) custom-call(f32[96,2048]{1,0:T(8,128)S(1)} %get-tuple-element.15.refs_0_, f32[96,2048]{1,0:T(8,128)S(1)} %get-tuple-element.16.refs_1_, f32[16,2048]{1,0:T(8,128)S(1)} %get-tuple-element.17.refs_2_, ...), custom_call_target="tpu_custom_call" | custom-call | tf_op jit(solution)/shard_map/pallas_call | solution.py:35

commit v3 on v2

--- a/solution.py
+++ b/solution.py
@@ -10,9 +10,62 @@
 MESH = pl.DeviceIdType.MESH
 LANES = 128
 PAIR = 2 * LANES
-RING = 4
-START_GATHER = 10
 VMEM_GRANT = 52 * 1024 * 1024
+
+
+ORDER = (
+    "F1 f1.6 f1.1 F2",
+    "F3 f1.0 F4 PM",
+    "P1.1 P1.0 P2.1 P2.0",
+    "f1.2 f2.0 P3.1 f2.6",
+    "f2.1 P3.0 f1.3 f3.0",
+    "P4 f2.3 f3.6 f1.4",
+    "f2.2 Q1 f2.4 f3.1",
+    "f3.2 Q2 f4.0 f3.4",
+    "f3.3 Q3 f4.2 f1.5",
+    "Q4 g1.2 f2.5 f4.1",
+    "g1.1 f1.7 f3.5 f4.4",
+    "g1.4 g2.2 f2.7 g2.1",
+    "g1.0 f3.7 f4.6 f4.5",
+    "g2.4 g1.5 f4.3 g3.1",
+    "g1.3 g1.6 f4.7 g3.4",
+    "g2.5 g4.1 g2.0 g1.7",
+    "g4.4 g2.3 g3.0 g3.2",
+    "g2.6 g4.2 g2.7 g3.5",
+    "g3.6 g3.3 g3.7 g4.3",
+    "g4.5 g4.6 g4.7 g4.0",
+)
+Z_SCATTER = (1,)
+Z_GATHER = (0,)
+
+
+def order_for(NP):
+    if NP == 8:
+        return [(a[:2], int(a[3:])) if "." in a else (a,) for line in ORDER for a in line.split()]
+    events = {
+        1: "F2", 2: "F3", 3: "F4 PM P1.0 P1.1", 4: "P2.0 P2.1", 5: "P3.0 P3.1",
+        6: "P4", 7: "Q1", 8: "Q2", 9: "Q3", 10: "Q4",
+    }
+    lags = {"f1": 0, "f2": 1, "f3": 2, "f4": 3, "g1": 10, "g2": 11, "g3": 12, "g4": 13}
+    order = [("F1",)]
+    for i in range(max(NP, 1) + 14):
+        for a in events.get(i, "").split():
+            order.append((a[:2], int(a[3:])) if "." in a else (a,))
+        order += [(name, i - lag) for name, lag in lags.items() if 0 <= i - lag < NP]
+    return order
+
+
+def z_pairs(NP):
+    return (Z_SCATTER, Z_GATHER) if NP == 8 else ((), ())
+
+
+def live_pairs(NP):
+    live, most = 0, 0
+    z_scatter = z_pairs(NP)[0]
+    for name, *p in order_for(NP):
+        live += (name == "f1") - (name in ("f3", "f4") and (name == "f4") == (p[0] in z_scatter))
+        most = max(most, live)
+    return most
 
 
 def contract_rows(left, right):
@@ -44,15 +97,16 @@
 
 def fused_kernel(
     Z, R, T,
-    m_ref, o_ref, f_ref, w_ref, m1_ref, m2_ref,
+    m_hbm, o_hbm, f_hbm, w_hbm, m1_hbm, m2_hbm,
     nw_ref, upd_ref, nf_ref, ns_ref, wc_ref,
-    mt, own, s1, r1, s2, r2, s3, r3,
+    m_ref, o_ref, f_ref, w_ref, m1_ref, m2_ref, load,
+    mt, own, s1, r1, s2, r2, s3, r3, rz,
     f_all, ft, yt, own_p, s1_p, r1_p, s2_p, r2_p, s3_p, r3_p, proj, q_all, q_own,
     stat, stat_all, ratio,
     t_send, t_recv, u_send, u_recv, v_send, v_recv,
     tp_send, tp_recv, up_send, up_recv, vp_send, vp_recv,
     gz_send, gz_recv, gx_send, gx_recv,
-    st_send, st_recv,
+    st_send, st_recv, cross_send, cross_recv,
 ):
     N = Z * R
     z, r, t = lax.axis_index("fs"), lax.axis_index("rep"), lax.axis_index("tp")
@@ -62,7 +116,6 @@
     FR, RK = f_ref.shape
     MR = m1_ref.shape[0]
     NP = CW // PAIR
-    K = START_GATHER
     HALF = CW // 2
     xn, yn, dn = r + 1 - 2 * lax.rem(r, 2), lax.rem(r + 2, R), R - 1 - r
     near = ((xn, yn), (yn, xn))
@@ -83,6 +136,26 @@
             return carry
 
         lax.fori_loop(1, Z, step, 0)
+
+    def fetch(src, dst, index):
+        return pltpu.make_async_copy(src, dst, load.at[index])
+
+    loads = {"f": fetch(f_hbm, f_ref, 0)}
+    for i in range(DH // PAIR):
+        part = pl.ds(i * PAIR, PAIR)
+        loads["m", i] = fetch(m_hbm.at[:, part], m_ref.at[:, part], len(loads))
+    for i in range(NP):
+        part = pl.ds(i * PAIR, PAIR)
+        loads["o", i] = fetch(o_hbm.at[:, part], o_ref.at[:, part], len(loads))
+    for name, src, dst in (("m1", m1_hbm, m1_ref), ("m2", m2_hbm, m2_ref), ("w", w_hbm, w_ref)):
+        loads[name] = fetch(src, dst, len(loads))
+    for copy in loads.values():
+        copy.start()
+
+    def need(*names):
+        for name in names:
+            if name in loads:
+                loads.pop(name).wait()
 
     barrier = pltpu.get_barrier_semaphore()
 
@@ -96,11 +169,10 @@
 
     lax.fori_loop(1, N * T, greet, 0)
 
-    def turn(i, carry):
-        mt[lanes(i, PAIR), :] = m_ref[:, lanes(i, PAIR)].T
-        return carry
-
-    lax.fori_loop(0, DH // PAIR, turn, 0)
+    for i in range(DH // PAIR):
+        need(("m", i))
+        mt[i * PAIR : (i + 1) * PAIR, :] = m_ref[:, i * PAIR : (i + 1) * PAIR].T
+    need("f")
 
     def move(src, dst, ss, rs, where):
         return pltpu.make_async_remote_copy(
@@ -173,19 +245,19 @@
             each_z(lambda zz: self.third(zz, z).wait_send())
 
     class Gather:
-        def __init__(self, g, h, ref, cols):
-            self.g, self.ref, self.cols = g, ref, cols
+        def __init__(self, g, h, ref, cols, rows=slice(None)):
+            self.g, self.ref, self.cols, self.rows = g, ref, cols, rows
             self.n1, self.n2 = near[h]
 
         def along(self, zz, src_z, block=None):
-            place = self.ref.at[src_z, r, :, self.cols]
+            place = self.ref.at[src_z, r, self.rows, self.cols]
             return move(
                 place if block is None else block, place,
                 gz_send.at[self.g, zz], gz_recv.at[self.g, src_z], device(zz, r, t),
             )
 
         def beside(self, k, rr):
-            place = self.ref.at[:, rr, :, self.cols]
+            place = self.ref.at[:, rr, self.rows, self.cols]
             to = self.n2 if k == 0 else self.n1
             return move(place, place, gx_send.at[self.g, k], gx_recv.at[self.g, k], device(z, to, t))
 
@@ -209,34 +281,122 @@
             self.beside(1, r).wait_send()
             self.beside(2, self.n2).wait_send()
 
+    class ScatterZ(Scatter):
+        def far(self, zz, src):
+            c = self.c
+            return move(
+                self.s1.at[c, :, zz], rz.at[along_z[c], src], self.vs.at[c, zz], self.vr.at[c, src], device(zz, r, t)
+            )
+
+        def first(self, k):
+            rr = self.n1 if k else dn
+            c = self.c
+            return move(self.s2.at[c, rr], self.r2.at[c, k], self.ts.at[c, k], self.tr.at[c, k], device(z, self.n1, t))
+
+        def second(self):
+            c = self.c
+            return move(self.s3.at[c, 0], self.r3.at[c, 0], self.us.at[c], self.ur.at[c], device(z, self.n2, t))
+
+        def stage1(self):
+            each_z(lambda zz: self.far(zz, z).start())
+
+        def stage2(self):
+            each_z(lambda zz: self.far(zz, zz).wait_recv())
+
+            def add(rr, carry):
+                total = self.mine(rr, z)
+                for e in range(1, Z):
+                    total = total + rz[along_z[self.c], other(e), rr].astype(f32)
+                self.own[self.slot, self.h, rr, z] = total
+                self.s2[self.c, rr] = total.astype(bf16)
+                return carry
+
+            lax.fori_loop(0, R, add, 0)
+            self.first(0).start()
+            self.first(1).start()
+
+        def stage3(self, put):
+            c = self.c
+            self.first(0).wait_recv()
+            self.s3[c, 0] = (self.mine(self.n2, z) + self.r2[c, 0].astype(f32)).astype(bf16)
+            self.second().start()
+
+        def last(self, get, put):
+            c = self.c
+            self.first(1).wait_recv()
+            self.second().wait_recv()
+            put(self.mine(r, z) + self.r2[c, 1].astype(f32) + self.r3[c, 0].astype(f32))
+
+        def sent(self):
+            self.first(0).wait_send()
+            self.first(1).wait_send()
+            self.second().wait_send()
+            each_z(lambda zz: self.far(zz, z).wait_send())
+
+    class GatherZ(Gather):
+        def along(self, zz, src_z):
+            place = self.ref.at[src_z, :, :, self.cols]
+            return move(place, place, gz_send.at[self.g, zz], gz_recv.at[self.g, src_z], device(zz, r, t))
+
+        def beside(self, k, rr):
+            place = self.ref.at[z, rr, :, self.cols]
+            to = self.n2 if k == 0 else self.n1
+            return move(place, place, gx_send.at[self.g, k], gx_recv.at[self.g, k], device(z, to, t))
+
+        def stage1(self):
+            self.beside(0, r).start()
+            self.beside(1, r).start()
+
+        def stage2(self):
+            self.beside(0, self.n2).wait_recv()
+            self.beside(2, self.n2).start()
+
+        def stage3(self):
+            self.beside(1, self.n1).wait_recv()
+            self.beside(2, dn).wait_recv()
+            each_z(lambda zz: self.along(zz, z).start())
+
+        def done(self):
+            each_z(lambda zz: self.along(zz, zz).wait_recv())
+            each_z(lambda zz: self.along(zz, z).wait_send())
+            self.beside(0, r).wait_send()
+            self.beside(1, r).wait_send()
+            self.beside(2, self.n2).wait_send()
+
     main_refs = (own, s1, r1, s2, r2, s3, r3)
     main_sems = (t_send, t_recv, u_send, u_recv, v_send, v_recv)
     proj_refs = (own_p, s1_p, r1_p, s2_p, r2_p, s3_p, r3_p)
     proj_sems = (tp_send, tp_recv, up_send, up_recv, vp_send, vp_recv)
 
+    slots = {}
+    z_scatter, z_gather = z_pairs(NP)
+    along_z = {2 * p + h: 2 * i + h for i, p in enumerate(z_scatter) for h in (0, 1)}
+
     def scatter(p, h):
-        return Scatter(2 * p + h, h, lax.rem(p, RING), main_refs, main_sems)
+        kind = ScatterZ if p in z_scatter else Scatter
+        return kind(2 * p + h, h, slots[p], main_refs, main_sems)
 
     def scatter_p(h):
         return Scatter(h, h, 0, proj_refs, proj_sems)
 
     def gather_w(p, h):
-        return Gather(2 * p + h, h, wc_ref, lanes(2 * p + h, LANES))
+        kind = GatherZ if p in z_gather else Gather
+        return kind(2 * p + h, h, wc_ref, lanes(2 * p + h, LANES))
 
     def gather_f(h):
-        return Gather(2 * NP + h, h, f_all, pl.ds(h * (RK // 2), RK // 2))
+        return Gather(2 * NP + h, h, f_all, pl.ds(h * (RK // 2), RK // 2), share)
 
     def gather_q(h):
         return Gather(2 * NP + 2 + h, h, q_all, pl.ds(h * HALF, HALF))
 
-    f_all[z, r] = f_ref[...]
+    share = pl.ds(pl.multiple_of(t * (FR // T), FR // T), FR // T)
+    f_all[z, r, share] = f_ref[share, :]
     pl.semaphore_wait(barrier, N * T - 1)
-    for h in (0, 1):
-        gather_f(h).stage1(f_ref.at[:, pl.ds(h * (RK // 2), RK // 2)])
 
     def product(p):
+        need(("o", p))
         cols = lanes(p, PAIR)
-        slot = lax.rem(p, RING)
+        slot = slots[p]
         G = R * FR
 
         def tile(zz, carry):
@@ -250,11 +410,27 @@
             return carry
 
         lax.fori_loop(0, Z, tile, 0)
+        if p in z_scatter:
+            both(lambda h: scatter(p, h).stage1())
+            return
         for k in (0, 1):
             for h in (0, 1):
                 scatter(p, h).first(k).start()
 
-    def project():
+    def start_factors():
+        for h in (0, 1):
+            gather_f(h).stage1(f_ref.at[share, pl.ds(h * (RK // 2), RK // 2)])
+
+    def swap_factors():
+        place = f_all.at[:, :, share, :]
+        return move(place, place, cross_send, cross_recv, device(z, r, 1 - t))
+
+    def finish_factors():
+        both(lambda h: gather_f(h).done())
+        swap_factors().start()
+
+    def low_rank():
+        swap_factors().wait()
         ft[...] = f_all[...].reshape(DH, RK).T
 
         def low(i, carry):
@@ -265,10 +441,12 @@
 
         lax.fori_loop(0, TOK // PAIR, low, 0)
 
+    def project(h):
+        need(*[("o", h * (NP // 2) + n) for n in range(NP // 2)])
+
         def tile(n, carry):
-            value = jnp.dot(yt[...], o_ref[:, lanes(n, PAIR)], preferred_element_type=f32)
-            h = n // (NP // 2)
-            cols = lanes(lax.rem(n, NP // 2), PAIR)
+            value = jnp.dot(yt[...], o_ref[:, lanes(h * (NP // 2) + n, PAIR)], preferred_element_type=f32)
+            cols = lanes(n, PAIR)
             for zz in range(Z):
                 for rr in range(R):
                     low_row = (zz * R + rr) * MR
@@ -277,7 +455,9 @@
                     s1_p[h, rr, zz, :, cols] = block.astype(bf16)
             return carry
 
-        lax.fori_loop(0, NP, tile, 0)
+        lax.fori_loop(0, NP // 2, tile, 0)
+        for k in (0, 1):
+            scatter_p(h).first(k).start()
 
     def s_copy(p, slot_of):
         q = lax.rem(every + p, N * T)
@@ -296,6 +476,7 @@
         return jnp.broadcast_to(total, (8, LANES))
 
     def moments():
+        need("m1", "m2")
         projected = proj[...]
         new_first = 0.8 * m1_ref[...] + 0.2 * projected
         new_second = 0.9 * m2_ref[...] + 0.1 * projected * projected
@@ -345,28 +526,9 @@
         for h in (0, 1):
             action(h)
 
-    def event_project():
-        both(lambda h: gather_f(h).done())
-        project()
-        for k in (0, 1):
-            both(lambda h: scatter_p(h).first(k).start())
-
-    def event_moments():
+    def finish_moments():
         both(lambda h: scatter_p(h).last(get_proj(h), put_proj(h)))
         moments()
-
-    events = {
-        1: lambda: both(lambda h: gather_f(h).stage2()),
-        2: lambda: both(lambda h: gather_f(h).stage3()),
-        3: event_project,
-        4: lambda: both(lambda h: scatter_p(h).stage2()),
-        5: lambda: both(lambda h: scatter_p(h).stage3(put_proj(h))),
-        6: event_moments,
-        7: combine,
-        8: lambda: both(lambda h: gather_q(h).stage2()),
-        9: lambda: both(lambda h: gather_q(h).stage3()),
-        10: lambda: both(lambda h: (gather_q(h).done(), scatter_p(h).sent())),
-    }
 
     def put_grad(p, h):
         def put(value):
@@ -378,6 +540,7 @@
         return lambda: upd_ref[:, lanes(2 * p + h, LANES)]
 
     def update(p):
+        need("w")
         cols = lanes(p, PAIR)
         mixed = q_all[:, :, :, cols].reshape(RK, PAIR)
         value = jnp.dot(f_ref[...], mixed, preferred_element_type=f32) + ratio[0:1, :] * upd_ref[:, cols]
@@ -387,26 +550,48 @@
         wc_ref[z, r, :, cols] = new_weight.astype(bf16)
         both(lambda h: gather_w(p, h).stage1())
 
-    def tick(i, carry):
-        def within(lag, action):
-            @pl.when((i >= lag) & (i < lag + NP))
-            def _():
-                action(i - lag)
-
-        for when, action in events.items():
-            pl.when(i == when)(action)
-        within(0, product)
-        within(1, lambda p: both(lambda h: scatter(p, h).stage2()))
-        within(2, lambda p: both(lambda h: scatter(p, h).stage3(put_grad(p, h))))
-        within(3, lambda p: both(lambda h: scatter(p, h).last(get_grad(p, h), put_grad(p, h))))
-        within(4, lambda p: both(lambda h: scatter(p, h).sent()))
-        within(K, update)
-        within(K + 1, lambda p: both(lambda h: gather_w(p, h).stage2()))
-        within(K + 2, lambda p: both(lambda h: gather_w(p, h).stage3()))
-        within(K + 3, lambda p: both(lambda h: gather_w(p, h).done()))
-        return carry
-
-    lax.fori_loop(0, NP + K + 3, tick, 0)
+    single = {
+        "F1": start_factors,
+        "F2": lambda: both(lambda h: gather_f(h).stage2()),
+        "F3": lambda: both(lambda h: gather_f(h).stage3()),
+        "F4": finish_factors,
+        "PM": low_rank,
+        "P4": finish_moments,
+        "Q1": combine,
+        "Q2": lambda: both(lambda h: gather_q(h).stage2()),
+        "Q3": lambda: both(lambda h: gather_q(h).stage3()),
+        "Q4": lambda: both(lambda h: gather_q(h).done()),
+    }
+    indexed = {
+        "P1": project,
+        "P2": lambda h: scatter_p(h).stage2(),
+        "P3": lambda h: scatter_p(h).stage3(put_proj(h)),
+        "f1": product,
+        "f2": lambda p: both(lambda h: scatter(p, h).stage2()),
+        "f3": lambda p: both(lambda h: scatter(p, h).stage3(put_grad(p, h))),
+        "f4": lambda p: both(lambda h: scatter(p, h).last(get_grad(p, h), put_grad(p, h))),
+        "g1": update,
+        "g2": lambda p: both(lambda h: gather_w(p, h).stage2()),
+        "g3": lambda p: both(lambda h: gather_w(p, h).stage3()),
+        "g4": lambda p: both(lambda h: gather_w(p, h).done()),
+    }
+    free, issued = list(range(own.shape[0])), []
+    for name, *index in order_for(NP):
+        if not index:
+            single[name]()
+            continue
+        if name == "f1":
+            slots[index[0]] = free.pop(0)
+        indexed[name](index[0])
+        if name == ("f4" if index[0] in z_scatter else "f3"):
+            free.append(slots[index[0]])
+            issued.append(index[0])
+        if name == "g3" and issued:
+            p = issued.pop(0)
+            both(lambda h: scatter(p, h).sent())
+    for p in issued:
+        both(lambda h: scatter(p, h).sent())
+    both(lambda h: scatter_p(h).sent())
 
 
 def fused(Z, R, T, *args):
@@ -429,17 +614,20 @@
             pltpu.VMEM(first_moment.shape, f32),
             pltpu.VMEM((Z, R, FR, CW), bf16),
         ),
-        in_specs=[vmem] * 6,
+        in_specs=[pl.BlockSpec(memory_space=pltpu.HBM)] * 6,
         out_specs=(vmem,) * 5,
         scratch_shapes=[
+            *[pltpu.VMEM(a.shape, a.dtype) for a in args],
+            dma((DH // PAIR + CW // PAIR + 4,)),
             pltpu.VMEM((DH, TOK), bf16),
-            pltpu.VMEM((RING, 2, R, Z, FR, LANES), f32),
+            pltpu.VMEM((live_pairs(CW // PAIR), 2, R, Z, FR, LANES), f32),
             pltpu.VMEM((NC, R, Z, FR, LANES), bf16),
             pltpu.VMEM((NC, 2, Z, FR, LANES), bf16),
+            pltpu.VMEM((NC, max(Z, R), FR, LANES), bf16),
+            pltpu.VMEM((NC, max(Z, R), FR, LANES), bf16),
             pltpu.VMEM((NC, Z, FR, LANES), bf16),
             pltpu.VMEM((NC, Z, FR, LANES), bf16),
-            pltpu.VMEM((NC, Z, FR, LANES), bf16),
-            pltpu.VMEM((NC, Z, FR, LANES), bf16),
+            pltpu.VMEM((max(1, 2 * len(z_pairs(CW // PAIR)[0])), Z, R, FR, LANES), bf16),
             pltpu.VMEM((Z, R, FR, RK), bf16),
             pltpu.VMEM((RK, DH), bf16),
             pltpu.VMEM((RK, TOK), bf16),
@@ -459,7 +647,7 @@
             *pair(NC, 2), *pair(NC), *pair(NC, Z),
             *pair(2, 2), *pair(2), *pair(2, Z),
             *pair(NC + 4, Z), *pair(NC + 4, 3),
-            *pair(N * T),
+            *pair(N * T), dma, dma,
         ],
         compiler_params=pltpu.CompilerParams(
             collective_id=0, has_side_effects=True, vmem_limit_bytes=VMEM_GRANT
@@ -514,7 +702,10 @@
             and weight.shape[0] % 16 == 0
             and first_moment.shape[0] % 16 == 0
             and factors.shape[1] == PAIR
+            and weight.shape[0] % (16 * T) == 0
             and R == 4
+            and T == 2
+            and Z == R
             and Z > 1
         )
         return fused(Z, R, T, *args) if fits else plain(*args)

time: 162 us -> 143 us (0.88)
  Pallas kernels: 161 us -> 142 us
    pallas_call x1, Pallas kernels: 158 us -> 138 us  [fused(): pl.pallas_call(functools.partial(fused_kernel, Z, R, T), out_shape=(pltpu...]
where the time goes in v3:
time: 143 us; the launch traced here: 142 us
  Pallas kernels  142 us (99%)
    pallas_call x1, Pallas kernels, fused(): pl.pallas_call(functools.partial(fused_kernel, Z, R, T), out_shape=(pltpu...  138 us
    pallas_call x1, Pallas kernels, drain_out(): pl.pallas_call(drain_kernel, out_shape=tuple((jax.ShapeDtypeStruct(a.shap...  3.35 us

profile of v3, /device:TPU:0, one launch (start us, length us, event | category | flops | bytes accessed | tf_op | source)
XLA Modules:
  0.0 142.1 jit_solution(11314962917978804090)
XLA Ops:
  0.6 138.2 %shard_map.101 = (f32[96,2048]{1,0:T(8,128)S(1)}, f32[96,2048]{1,0:T(8,128)S(1)}, f32[16,2048]{1,0:T(8,128)S(1)}, f32[16,2048]{1,0:T(8,128)S(1)}, bf16[4,4,96,2048]{3,2,1,0:T(8,128)(2,1)S(1)}) custom-call(bf16[1024,1536]{1,0:T(8,128)(2,1)} %m_hbm.1, bf16[1024,2048]{1,0:T(8,128)(2,1)} %o_hbm.1, bf16[96,256]{1,0:T(8,128)(2,1)} %f_hbm.1, f32[96,2048]{1,0:T(8,128)} %w_hbm.1, ...), custom_call_target="tpu_custom_call" | custom-call | tf_op jit(solution)/shard_map/pallas_call | solution.py:608
  138.8 3.4 %shard_map.102 = (f32[96,2048]{1,0:T(8,128)}, f32[96,2048]{1,0:T(8,128)}, f32[16,2048]{1,0:T(8,128)}, f32[16,2048]{1,0:T(8,128)}, bf16[4,4,96,2048]{3,2,1,0:T(8,128)(2,1)}) custom-call(f32[96,2048]{1,0:T(8,128)S(1)} %get-tuple-element.15.refs_0_, f32[96,2048]{1,0:T(8,128)S(1)} %get-tuple-element.16.refs_1_, f32[16,2048]{1,0:T(8,128)S(1)} %get-tuple-element.17.refs_2_, ...), custom_call_target="tpu_custom_call" | custom-call | tf_op jit(solution)/shard_map/pallas_call | solution.py:88

commit v4 on v3

--- a/solution.py
+++ b/solution.py
@@ -14,43 +14,63 @@
 
 
 ORDER = (
-    "F1 f1.6 f1.1 F2",
-    "F3 f1.0 F4 PM",
-    "P1.1 P1.0 P2.1 P2.0",
-    "f1.2 f2.0 P3.1 f2.6",
-    "f2.1 P3.0 f1.3 f3.0",
-    "P4 f2.3 f3.6 f1.4",
-    "f2.2 Q1 f2.4 f3.1",
-    "f3.2 Q2 f4.0 f3.4",
-    "f3.3 Q3 f4.2 f1.5",
-    "Q4 g1.2 f2.5 f4.1",
-    "g1.1 f1.7 f3.5 f4.4",
-    "g1.4 g2.2 f2.7 g2.1",
-    "g1.0 f3.7 f4.6 f4.5",
-    "g2.4 g1.5 f4.3 g3.1",
-    "g1.3 g1.6 f4.7 g3.4",
-    "g2.5 g4.1 g2.0 g1.7",
-    "g4.4 g2.3 g3.0 g3.2",
-    "g2.6 g4.2 g2.7 g3.5",
-    "g3.6 g3.3 g3.7 g4.3",
-    "g4.5 g4.6 g4.7 g4.0",
+    "F1 f1.0 f1.1 F2",
+    "f2.0.1 f2.0.0 F3 f1.6",
+    "F4 f1.4 PM P1.0",
+    "P1.1 f3.0.1 f2.6.1 f3.0.0",
+    "P2.0 P2.1 f1.2 P3.0",
+    "f2.6.0 f4.0.0 f2.4.1 P3.1",
+    "f2.1.1 f1.3 f3.6.1 f3.4.1",
+    "f2.2.1 f2.4.0 P4 f4.0.1",
+    "f3.1.1 f1.5 f3.4.0 f2.3.0",
+    "f3.2.1 f2.2.0 f2.3.1 Q1",
+    "f2.5.0 f1.7 f3.2.0 f2.5.1",
+    "f4.2.1 f3.3.0 Q2.1 f3.6.0",
+    "f4.6.1 f2.1.0 Q2.0 f3.3.1",
+    "f4.1.1 f4.4.1 f3.5.1 f2.7.0",
+    "f3.1.0 Q3.1 Q3.0 f3.5.0",
+    "f3.7.0 f4.2.0 f2.7.1 f4.4.0",
+    "f4.5.1 f4.3.0 f4.1.0 Q4",
+    "g1.2 g1.1 g1.0 g1.4",
+    "f4.6.0 ga.2 f4.5.0 f4.3.1",
+    "g1.5 g2.0.1 g2.0.0 ga.1",
+    "g1.3 g2.2.1 f3.7.1 g2.2.0",
+    "ga.4 g2.3.0 g1.6 g2.1.1",
+    "g2.1.0 ga.5 g2.4.0 g3.0.0",
+    "g3.2.1 g2.3.1 f4.7.1 g2.4.1",
+    "ga.6 g2.5.0 f4.7.0 g1.7",
+    "g2.6.1 g3.3.0 g3.1.0 ga.0.0",
+    "g4.2.1 g3.4.1 g2.5.1 g3.3.1",
+    "g3.0.1 ga.7 g3.5.0 g4.1.0",
+    "ga.3.0 g2.6.0 g3.5.1 g3.4.0",
+    "g2.7.0 g2.7.1 g4.5.0 g3.1.1",
+    "g3.6.0 ga.3.1 g3.6.1 g4.4.0",
+    "g3.7.0 ga.0.1 g4.3.0 g4.0.0",
+    "g3.2.0 g4.4.1 g3.7.1 g4.6.0",
+    "g4.3.1 g4.7.0 g4.5.1 g4.1.1",
+    "g4.6.1 g4.0.1 g4.2.0 g4.7.1",
 )
 Z_SCATTER = (1,)
-Z_GATHER = (0,)
+Z_GATHER = (0, 3)
+
+
+def token(text):
+    name, *index = text.split(".")
+    return (name, *map(int, index))
 
 
 def order_for(NP):
     if NP == 8:
-        return [(a[:2], int(a[3:])) if "." in a else (a,) for line in ORDER for a in line.split()]
+        return [token(a) for line in ORDER for a in line.split()]
     events = {
         1: "F2", 2: "F3", 3: "F4 PM P1.0 P1.1", 4: "P2.0 P2.1", 5: "P3.0 P3.1",
         6: "P4", 7: "Q1", 8: "Q2", 9: "Q3", 10: "Q4",
     }
-    lags = {"f1": 0, "f2": 1, "f3": 2, "f4": 3, "g1": 10, "g2": 11, "g3": 12, "g4": 13}
+    lags = {"f1": 0, "f2": 1, "f3": 2, "f4": 3, "g1": 10, "ga": 11, "g2": 11, "g3": 12, "g4": 13}
     order = [("F1",)]
     for i in range(max(NP, 1) + 14):
         for a in events.get(i, "").split():
-            order.append((a[:2], int(a[3:])) if "." in a else (a,))
+            order.append(token(a))
         order += [(name, i - lag) for name, lag in lags.items() if 0 <= i - lag < NP]
     return order
 
@@ -60,10 +80,14 @@
 
 
 def live_pairs(NP):
-    live, most = 0, 0
+    live, most, passed = 0, 0, {}
     z_scatter = z_pairs(NP)[0]
-    for name, *p in order_for(NP):
-        live += (name == "f1") - (name in ("f3", "f4") and (name == "f4") == (p[0] in z_scatter))
+    for name, *index in order_for(NP):
+        live += name == "f1"
+        if index and name == ("f4" if index[0] in z_scatter else "f3"):
+            p = index[0]
+            passed[p] = passed.get(p, 0) + (1 if index[1:] else 2)
+            live -= passed[p] == 2
         most = max(most, live)
     return most
 
@@ -105,7 +129,7 @@
     stat, stat_all, ratio,
     t_send, t_recv, u_send, u_recv, v_send, v_recv,
     tp_send, tp_recv, up_send, up_recv, vp_send, vp_recv,
-    gz_send, gz_recv, gx_send, gx_recv,
+    gz_send, gz_recv, gx_send, gx_recv, gf_send,
     st_send, st_recv, cross_send, cross_recv,
 ):
     N = Z * R
@@ -119,6 +143,11 @@
     HALF = CW // 2
     xn, yn, dn = r + 1 - 2 * lax.rem(r, 2), lax.rem(r + 2, R), R - 1 - r
     near = ((xn, yn), (yn, xn))
+    low_half = z < 2
+    twin = z + 1 - 2 * lax.rem(z, 2)
+    cross = jnp.where(low_half, 2, 1)
+    away = jnp.where(low_half, 2, 0)
+    middle = (z == 1) | (z == 2)
     f32, bf16 = jnp.float32, jnp.bfloat16
 
     def device(zz, rr, tt):
@@ -159,15 +188,13 @@
 
     barrier = pltpu.get_barrier_semaphore()
 
-    def greet(p, carry):
-        q = lax.rem(every + p, N * T)
-        d = q // T
-        pl.semaphore_signal(
-            barrier, inc=1, device_id=device(d // R, lax.rem(d, R), lax.rem(q, T)), device_id_type=MESH
-        )
-        return carry
-
-    lax.fori_loop(1, N * T, greet, 0)
+    def greet(zz, rr, tt):
+        pl.semaphore_signal(barrier, inc=1, device_id=device(zz, rr, tt), device_id_type=MESH)
+
+    each_z(lambda zz: greet(zz, r, t))
+    greet(z, xn, t)
+    greet(z, yn, t)
+    greet(z, r, 1 - t)
 
     for i in range(DH // PAIR):
         need(("m", i))
@@ -249,11 +276,11 @@
             self.g, self.ref, self.cols, self.rows = g, ref, cols, rows
             self.n1, self.n2 = near[h]
 
-        def along(self, zz, src_z, block=None):
+        def along(self, zz, src_z, block=None, sent=None):
             place = self.ref.at[src_z, r, self.rows, self.cols]
             return move(
                 place if block is None else block, place,
-                gz_send.at[self.g, zz], gz_recv.at[self.g, src_z], device(zz, r, t),
+                gz_send.at[self.g, zz] if sent is None else sent, gz_recv.at[self.g, src_z], device(zz, r, t),
             )
 
         def beside(self, k, rr):
@@ -264,8 +291,42 @@
         def stage1(self, block=None):
             each_z(lambda zz: self.along(zz, z, block).start())
 
-        def stage2(self):
-            each_z(lambda zz: self.along(zz, zz).wait_recv())
+        def spread(self):
+            self.along(cross, z).start()
+            self.along(twin, z).start()
+
+        def onward(self, k):
+            return self.along(twin, away + k, None, gf_send.at[self.g, k])
+
+        def forward(self):
+            @pl.when(middle)
+            def _():
+                for k in (0, 1):
+                    self.along(twin, away + k).wait_recv()
+                    self.onward(k).start()
+
+        def gathered(self):
+            self.along(twin, twin).wait_recv()
+
+            @pl.when(jnp.logical_not(middle))
+            def _():
+                for k in (0, 1):
+                    self.along(twin, away + k).wait_recv()
+
+        def spread_sent(self):
+            self.along(cross, z).wait_send()
+            self.along(twin, z).wait_send()
+
+            @pl.when(middle)
+            def _():
+                for k in (0, 1):
+                    self.onward(k).wait_send()
+
+        def stage2(self, spread=False):
+            if spread:
+                self.gathered()
+            else:
+                each_z(lambda zz: self.along(zz, zz).wait_recv())
             self.beside(0, r).start()
             self.beside(1, r).start()
 
@@ -273,10 +334,13 @@
             self.beside(0, self.n2).wait_recv()
             self.beside(2, self.n2).start()
 
-        def done(self):
+        def done(self, spread=False):
             self.beside(1, self.n1).wait_recv()
             self.beside(2, dn).wait_recv()
-            each_z(lambda zz: self.along(zz, z).wait_send())
+            if spread:
+                self.spread_sent()
+            else:
+                each_z(lambda zz: self.along(zz, z).wait_send())
             self.beside(0, r).wait_send()
             self.beside(1, r).wait_send()
             self.beside(2, self.n2).wait_send()
@@ -334,31 +398,34 @@
             each_z(lambda zz: self.far(zz, z).wait_send())
 
     class GatherZ(Gather):
-        def along(self, zz, src_z):
+        def along(self, zz, src_z, block=None, sent=None):
             place = self.ref.at[src_z, :, :, self.cols]
-            return move(place, place, gz_send.at[self.g, zz], gz_recv.at[self.g, src_z], device(zz, r, t))
+            return move(
+                place, place, gz_send.at[self.g, zz] if sent is None else sent, gz_recv.at[self.g, src_z],
+                device(zz, r, t),
+            )
 
         def beside(self, k, rr):
             place = self.ref.at[z, rr, :, self.cols]
             to = self.n2 if k == 0 else self.n1
             return move(place, place, gx_send.at[self.g, k], gx_recv.at[self.g, k], device(z, to, t))
 
-        def stage1(self):
+        def begin(self):
             self.beside(0, r).start()
             self.beside(1, r).start()
 
-        def stage2(self):
+        def stage2(self, spread=True):
             self.beside(0, self.n2).wait_recv()
             self.beside(2, self.n2).start()
 
         def stage3(self):
             self.beside(1, self.n1).wait_recv()
             self.beside(2, dn).wait_recv()
-            each_z(lambda zz: self.along(zz, z).start())
-
-        def done(self):
-            each_z(lambda zz: self.along(zz, zz).wait_recv())
-            each_z(lambda zz: self.along(zz, z).wait_send())
+            self.spread()
+
+        def done(self, spread=True):
+            self.gathered()
+            self.spread_sent()
             self.beside(0, r).wait_send()
             self.beside(1, r).wait_send()
             self.beside(2, self.n2).wait_send()
@@ -391,7 +458,7 @@
 
     share = pl.ds(pl.multiple_of(t * (FR // T), FR // T), FR // T)
     f_all[z, r, share] = f_ref[share, :]
-    pl.semaphore_wait(barrier, N * T - 1)
+    pl.semaphore_wait(barrier, Z + 2)
 
     def product(p):
         need(("o", p))
@@ -473,7 +540,7 @@
         total = row[:, :LANES]
         for j in range(1, CW // LANES):
             total = total + row[:, j * LANES : (j + 1) * LANES]
-        return jnp.broadcast_to(total, (8, LANES))
+        return total
 
     def moments():
         need("m1", "m2")
@@ -484,8 +551,8 @@
         ns_ref[...] = new_second
         dir_wide = (new_first / (jnp.sqrt(new_second) + 1e-08)).astype(bf16).astype(f32)
         proj_wide = projected.astype(bf16).astype(f32)
-        stat[0] = fold(dir_wide * dir_wide)
-        stat[1] = fold(proj_wide * proj_wide)
+        stat[0:1, :] = fold(dir_wide * dir_wide)
+        stat[1:2, :] = fold(proj_wide * proj_wide)
         stat_all[every] = stat[...]
 
         def send(p, carry):
@@ -501,8 +568,8 @@
 
         lax.fori_loop(1, N * T, wait, 0)
         totals = jnp.sum(stat_all[...], axis=0)
-        dir_sum = jnp.sum(totals[0, 0:1, :], axis=1, keepdims=True)
-        proj_sum = jnp.sum(totals[1, 0:1, :], axis=1, keepdims=True)
+        dir_sum = jnp.sum(totals[0:1, :], axis=1, keepdims=True)
+        proj_sum = jnp.sum(totals[1:2, :], axis=1, keepdims=True)
         scale_ratio = jnp.sqrt(dir_sum) / jnp.sqrt(proj_sum + 1e-06)
         ratio[...] = jnp.broadcast_to(scale_ratio, (8, PAIR))
         projected = proj[...]
@@ -548,7 +615,10 @@
         new_weight = w_ref[:, cols] - 0.01 * value
         nw_ref[:, cols] = new_weight
         wc_ref[z, r, :, cols] = new_weight.astype(bf16)
-        both(lambda h: gather_w(p, h).stage1())
+        if p in z_gather:
+            both(lambda h: gather_w(p, h).begin())
+        else:
+            both(lambda h: gather_w(p, h).spread())
 
     single = {
         "F1": start_factors,
@@ -558,37 +628,49 @@
         "PM": low_rank,
         "P4": finish_moments,
         "Q1": combine,
-        "Q2": lambda: both(lambda h: gather_q(h).stage2()),
-        "Q3": lambda: both(lambda h: gather_q(h).stage3()),
         "Q4": lambda: both(lambda h: gather_q(h).done()),
     }
-    indexed = {
+    halves = {
         "P1": project,
         "P2": lambda h: scatter_p(h).stage2(),
         "P3": lambda h: scatter_p(h).stage3(put_proj(h)),
-        "f1": product,
-        "f2": lambda p: both(lambda h: scatter(p, h).stage2()),
-        "f3": lambda p: both(lambda h: scatter(p, h).stage3(put_grad(p, h))),
-        "f4": lambda p: both(lambda h: scatter(p, h).last(get_grad(p, h), put_grad(p, h))),
-        "g1": update,
-        "g2": lambda p: both(lambda h: gather_w(p, h).stage2()),
-        "g3": lambda p: both(lambda h: gather_w(p, h).stage3()),
-        "g4": lambda p: both(lambda h: gather_w(p, h).done()),
+        "Q2": lambda h: gather_q(h).stage2(),
+        "Q3": lambda h: gather_q(h).stage3(),
     }
-    free, issued = list(range(own.shape[0])), []
+    pairs = {"f1": product, "g1": update}
+    chunks = {
+        "f2": lambda p, h: scatter(p, h).stage2(),
+        "f3": lambda p, h: scatter(p, h).stage3(put_grad(p, h)),
+        "f4": lambda p, h: scatter(p, h).last(get_grad(p, h), put_grad(p, h)),
+        "ga": lambda p, h: gather_w(p, h).forward(),
+        "g2": lambda p, h: gather_w(p, h).stage2(True),
+        "g3": lambda p, h: gather_w(p, h).stage3(),
+        "g4": lambda p, h: gather_w(p, h).done(True),
+    }
+    free, issued, passed = list(range(own.shape[0])), [], {}
     for name, *index in order_for(NP):
-        if not index:
+        if name in single:
             single[name]()
-            continue
-        if name == "f1":
-            slots[index[0]] = free.pop(0)
-        indexed[name](index[0])
-        if name == ("f4" if index[0] in z_scatter else "f3"):
-            free.append(slots[index[0]])
-            issued.append(index[0])
-        if name == "g3" and issued:
-            p = issued.pop(0)
-            both(lambda h: scatter(p, h).sent())
+        elif name in halves:
+            for h in index or (0, 1):
+                halves[name](h)
+        elif name in pairs:
+            p = index[0]
+            if name == "f1":
+                slots[p] = free.pop(0)
+            pairs[name](p)
+        else:
+            p = index[0]
+            for h in index[1:] or (0, 1):
+                chunks[name](p, h)
+                if name == ("f4" if p in z_scatter else "f3"):
+                    passed[p] = passed.get(p, 0) + 1
+                    if passed[p] == 2:
+                        free.append(slots[p])
+                        issued.append(p)
+            if name == "g3" and issued:
+                p = issued.pop(0)
+                both(lambda h: scatter(p, h).sent())
     for p in issued:
         both(lambda h: scatter(p, h).sent())
     both(lambda h: scatter_p(h).sent())
@@ -641,12 +723,12 @@
             pltpu.VMEM((MR, CW), f32),
             pltpu.VMEM((Z, R, MR, CW), bf16),
             pltpu.VMEM((MR, CW), bf16),
-            pltpu.VMEM((2, 8, LANES), f32),
-            pltpu.VMEM((N * T, 2, 8, LANES), f32),
+            pltpu.VMEM((2, LANES), f32),
+            pltpu.VMEM((N * T, 2, LANES), f32),
             pltpu.VMEM((8, PAIR), f32),
             *pair(NC, 2), *pair(NC), *pair(NC, Z),
             *pair(2, 2), *pair(2), *pair(2, Z),
-            *pair(NC + 4, Z), *pair(NC + 4, 3),
+            *pair(NC + 4, Z), *pair(NC + 4, 3), dma((NC + 4, 2)),
             *pair(N * T), dma, dma,
         ],
         compiler_params=pltpu.CompilerParams(

time: 143 us -> 134 us (0.937)
  Pallas kernels: 142 us -> 133 us
    pallas_call x1, Pallas kernels: 138 us -> 130 us  [fused(): pl.pallas_call(functools.partial(fused_kernel, Z, R, T), out_shape=(pltpu...]
where the time goes in v4:
time: 134 us
  Pallas kernels  133 us (99%)
    pallas_call x1, Pallas kernels, fused(): pl.pallas_call(functools.partial(fused_kernel, Z, R, T), out_shape=(pltpu...  130 us
    pallas_call x1, Pallas kernels, drain_out(): pl.pallas_call(drain_kernel, out_shape=tuple((jax.ShapeDtypeStruct(a.shap...  3.35 us

profile of v4, /device:TPU:0, one launch (start us, length us, event | category | flops | bytes accessed | tf_op | source)
XLA Modules:
  0.0 133.5 jit_solution(7993589105717328813)
XLA Ops:
  0.6 129.5 %shard_map.101 = (f32[96,2048]{1,0:T(8,128)S(1)}, f32[96,2048]{1,0:T(8,128)S(1)}, f32[16,2048]{1,0:T(8,128)S(1)}, f32[16,2048]{1,0:T(8,128)S(1)}, bf16[4,4,96,2048]{3,2,1,0:T(8,128)(2,1)S(1)}) custom-call(bf16[1024,1536]{1,0:T(8,128)(2,1)} %m_hbm.1, bf16[1024,2048]{1,0:T(8,128)(2,1)} %o_hbm.1, bf16[96,256]{1,0:T(8,128)(2,1)} %f_hbm.1, f32[96,2048]{1,0:T(8,128)} %w_hbm.1, ...), custom_call_target="tpu_custom_call" | custom-call | tf_op jit(solution)/shard_map/pallas_call | solution.py:690
  130.2 3.4 %shard_map.102 = (f32[96,2048]{1,0:T(8,128)}, f32[96,2048]{1,0:T(8,128)}, f32[16,2048]{1,0:T(8,128)}, f32[16,2048]{1,0:T(8,128)}, bf16[4,4,96,2048]{3,2,1,0:T(8,128)(2,1)}) custom-call(f32[96,2048]{1,0:T(8,128)S(1)} %get-tuple-element.15.refs_0_, f32[96,2048]{1,0:T(8,128)S(1)} %get-tuple-element.16.refs_1_, f32[16,2048]{1,0:T(8,128)S(1)} %get-tuple-element.17.refs_2_, ...), custom_call_target="tpu_custom_call" | custom-call | tf_op jit(solution)/shard_map/pallas_call | solution.py:112

commit v5 on v4

--- a/solution.py
+++ b/solution.py
@@ -10,45 +10,50 @@
 MESH = pl.DeviceIdType.MESH
 LANES = 128
 PAIR = 2 * LANES
+PARTS = 4
 VMEM_GRANT = 52 * 1024 * 1024
 
 
 ORDER = (
-    "F1 f1.0 f1.1 F2",
-    "f2.0.1 f2.0.0 F3 f1.6",
-    "F4 f1.4 PM P1.0",
-    "P1.1 f3.0.1 f2.6.1 f3.0.0",
-    "P2.0 P2.1 f1.2 P3.0",
-    "f2.6.0 f4.0.0 f2.4.1 P3.1",
-    "f2.1.1 f1.3 f3.6.1 f3.4.1",
-    "f2.2.1 f2.4.0 P4 f4.0.1",
-    "f3.1.1 f1.5 f3.4.0 f2.3.0",
-    "f3.2.1 f2.2.0 f2.3.1 Q1",
-    "f2.5.0 f1.7 f3.2.0 f2.5.1",
-    "f4.2.1 f3.3.0 Q2.1 f3.6.0",
-    "f4.6.1 f2.1.0 Q2.0 f3.3.1",
-    "f4.1.1 f4.4.1 f3.5.1 f2.7.0",
-    "f3.1.0 Q3.1 Q3.0 f3.5.0",
-    "f3.7.0 f4.2.0 f2.7.1 f4.4.0",
-    "f4.5.1 f4.3.0 f4.1.0 Q4",
-    "g1.2 g1.1 g1.0 g1.4",
-    "f4.6.0 ga.2 f4.5.0 f4.3.1",
-    "g1.5 g2.0.1 g2.0.0 ga.1",
-    "g1.3 g2.2.1 f3.7.1 g2.2.0",
-    "ga.4 g2.3.0 g1.6 g2.1.1",
-    "g2.1.0 ga.5 g2.4.0 g3.0.0",
-    "g3.2.1 g2.3.1 f4.7.1 g2.4.1",
-    "ga.6 g2.5.0 f4.7.0 g1.7",
-    "g2.6.1 g3.3.0 g3.1.0 ga.0.0",
-    "g4.2.1 g3.4.1 g2.5.1 g3.3.1",
-    "g3.0.1 ga.7 g3.5.0 g4.1.0",
-    "ga.3.0 g2.6.0 g3.5.1 g3.4.0",
-    "g2.7.0 g2.7.1 g4.5.0 g3.1.1",
-    "g3.6.0 ga.3.1 g3.6.1 g4.4.0",
-    "g3.7.0 ga.0.1 g4.3.0 g4.0.0",
-    "g3.2.0 g4.4.1 g3.7.1 g4.6.0",
-    "g4.3.1 g4.7.0 g4.5.1 g4.1.1",
-    "g4.6.1 g4.0.1 g4.2.0 g4.7.1",
+    "F1 f1.4 f1.1 F2",
+    "f1.0 F3 f2.4.1 f1.6",
+    "F4 f2.0.1 f2.0.0 f2.4.0",
+    "f3.4.1 PM P1.3 P1.2",
+    "P1.1 P1.0 f3.0.1 f3.0.0",
+    "P2.3 P2.2 f1.2 f2.6.1",
+    "P2.0 P3.2 P3.3 f2.6.0",
+    "f3.4.0 f2.2.0 P2.1 f1.3",
+    "f2.1.1 P3.0 P3.1 f2.1.0",
+    "f3.6.1 f2.2.1 f3.2.0 f3.6.0",
+    "f2.3.1 f2.3.0 P4 f1.7",
+    "f3.3.0 f3.2.1 f1.5 Q1",
+    "f4.3.0 f2.7.0 f3.1.1 f2.7.1",
+    "f3.3.1 f4.4.1 f4.2.1 f4.6.1",
+    "Q2.0 f3.1.0 f4.1.1 f4.2.0",
+    "f4.4.0 Q2.1 f2.5.0 f3.7.1",
+    "Q3.0 f2.5.1 f4.6.0 Q2.3",
+    "f3.7.0 f4.0.1 Q3.1 f4.1.0",
+    "Q4.0 g1.1 f4.7.1 f4.3.1",
+    "Q2.2 f3.5.1 Q4.1 Q3.3",
+    "g1.2 f4.0.0 g1.3 ga.1",
+    "Q3.2 f4.7.0 Q4.3 g1.6",
+    "g2.3.0 g2.1.1 f3.5.0 ga.2",
+    "g1.0 g2.1.0 Q4.2 g1.4",
+    "g2.3.1 ga.6 f4.5.1 g2.2.1",
+    "g1.7 g2.2.0 f4.5.0 g1.5",
+    "g2.0.0 g3.3.0 g2.0.1 g2.6.1",
+    "ga.4 g3.2.1 g3.1.1 ga.7",
+    "g3.1.0 g2.6.0 g2.4.0 g3.0.1",
+    "ga.5 g3.6.1 g3.2.0 g2.7.0",
+    "g3.0.0 g2.5.0 g2.5.1 g2.7.1",
+    "g4.1.0 g3.3.1 g2.4.1 g3.6.0",
+    "ga.3.0 ga.0.1 g4.2.1 ga.0.0",
+    "g4.1.1 g4.3.0 g3.5.1 g3.4.0",
+    "g3.7.1 ga.3.1 g3.4.1 g3.5.0",
+    "g4.6.0 g3.7.0 g4.2.0 g4.6.1",
+    "g4.5.1 g4.0.0 g4.4.0 g4.0.1",
+    "g4.7.1 g4.5.0 g4.3.1 g4.7.0",
+    "g4.4.1",
 )
 Z_SCATTER = (1,)
 Z_GATHER = (0, 3)
@@ -63,7 +68,7 @@
     if NP == 8:
         return [token(a) for line in ORDER for a in line.split()]
     events = {
-        1: "F2", 2: "F3", 3: "F4 PM P1.0 P1.1", 4: "P2.0 P2.1", 5: "P3.0 P3.1",
+        1: "F2", 2: "F3", 3: "F4 PM P1", 4: "P2", 5: "P3",
         6: "P4", 7: "Q1", 8: "Q2", 9: "Q3", 10: "Q4",
     }
     lags = {"f1": 0, "f2": 1, "f3": 2, "f4": 3, "g1": 10, "ga": 11, "g2": 11, "g3": 12, "g4": 13}
@@ -140,7 +145,7 @@
     FR, RK = f_ref.shape
     MR = m1_ref.shape[0]
     NP = CW // PAIR
-    HALF = CW // 2
+    PART = CW // PARTS
     xn, yn, dn = r + 1 - 2 * lax.rem(r, 2), lax.rem(r + 2, R), R - 1 - r
     near = ((xn, yn), (yn, xn))
     low_half = z < 2
@@ -443,8 +448,8 @@
         kind = ScatterZ if p in z_scatter else Scatter
         return kind(2 * p + h, h, slots[p], main_refs, main_sems)
 
-    def scatter_p(h):
-        return Scatter(h, h, 0, proj_refs, proj_sems)
+    def scatter_p(c):
+        return Scatter(c, c % 2, c, proj_refs, proj_sems)
 
     def gather_w(p, h):
         kind = GatherZ if p in z_gather else Gather
@@ -453,8 +458,8 @@
     def gather_f(h):
         return Gather(2 * NP + h, h, f_all, pl.ds(h * (RK // 2), RK // 2), share)
 
-    def gather_q(h):
-        return Gather(2 * NP + 2 + h, h, q_all, pl.ds(h * HALF, HALF))
+    def gather_q(c):
+        return Gather(2 * NP + 2 + c, c % 2, q_all, pl.ds(c * PART, PART))
 
     share = pl.ds(pl.multiple_of(t * (FR // T), FR // T), FR // T)
     f_all[z, r, share] = f_ref[share, :]
@@ -508,23 +513,24 @@
 
         lax.fori_loop(0, TOK // PAIR, low, 0)
 
-    def project(h):
-        need(*[("o", h * (NP // 2) + n) for n in range(NP // 2)])
+    def project(c):
+        tiles = PART // PAIR
+        need(*[("o", c * tiles + n) for n in range(tiles)])
 
         def tile(n, carry):
-            value = jnp.dot(yt[...], o_ref[:, lanes(h * (NP // 2) + n, PAIR)], preferred_element_type=f32)
+            value = jnp.dot(yt[...], o_ref[:, lanes(c * tiles + n, PAIR)], preferred_element_type=f32)
             cols = lanes(n, PAIR)
             for zz in range(Z):
                 for rr in range(R):
                     low_row = (zz * R + rr) * MR
                     block = value[low_row : low_row + MR, :]
-                    own_p[0, h, rr, zz, :, cols] = block
-                    s1_p[h, rr, zz, :, cols] = block.astype(bf16)
+                    own_p[c, c % 2, rr, zz, :, cols] = block
+                    s1_p[c, rr, zz, :, cols] = block.astype(bf16)
             return carry
 
-        lax.fori_loop(0, NP // 2, tile, 0)
+        lax.fori_loop(0, tiles, tile, 0)
         for k in (0, 1):
-            scatter_p(h).first(k).start()
+            scatter_p(c).first(k).start()
 
     def s_copy(p, slot_of):
         q = lax.rem(every + p, N * T)
@@ -577,24 +583,25 @@
         mixed = (dir_wide - scale_ratio * projected.astype(bf16).astype(f32)).astype(bf16)
         q_own[...] = mixed
         q_all[z, r] = mixed
-        for h in (0, 1):
-            gather_q(h).stage1(q_own.at[:, pl.ds(h * HALF, HALF)])
-
-    def put_proj(h):
+        for c in range(PARTS):
+            gather_q(c).stage1(q_own.at[:, pl.ds(c * PART, PART)])
+
+    def put_proj(c):
         def put(value):
-            proj[:, h * HALF : (h + 1) * HALF] = value
+            proj[:, c * PART : (c + 1) * PART] = value
 
         return put
 
-    def get_proj(h):
-        return lambda: proj[:, h * HALF : (h + 1) * HALF]
+    def get_proj(c):
+        return lambda: proj[:, c * PART : (c + 1) * PART]
 
     def both(action):
         for h in (0, 1):
             action(h)
 
     def finish_moments():
-        both(lambda h: scatter_p(h).last(get_proj(h), put_proj(h)))
+        for c in range(PARTS):
+            scatter_p(c).last(get_proj(c), put_proj(c))
         moments()
 
     def put_grad(p, h):
@@ -628,14 +635,14 @@
         "PM": low_rank,
         "P4": finish_moments,
         "Q1": combine,
-        "Q4": lambda: both(lambda h: gather_q(h).done()),
     }
-    halves = {
+    parts = {
         "P1": project,
-        "P2": lambda h: scatter_p(h).stage2(),
-        "P3": lambda h: scatter_p(h).stage3(put_proj(h)),
-        "Q2": lambda h: gather_q(h).stage2(),
-        "Q3": lambda h: gather_q(h).stage3(),
+        "P2": lambda c: scatter_p(c).stage2(),
+        "P3": lambda c: scatter_p(c).stage3(put_proj(c)),
+        "Q2": lambda c: gather_q(c).stage2(),
+        "Q3": lambda c: gather_q(c).stage3(),
+        "Q4": lambda c: gather_q(c).done(),
     }
     pairs = {"f1": product, "g1": update}
     chunks = {
@@ -651,9 +658,9 @@
     for name, *index in order_for(NP):
         if name in single:
             single[name]()
-        elif name in halves:
-            for h in index or (0, 1):
-                halves[name](h)
+        elif name in parts:
+            for c in index or range(PARTS):
+                parts[name](c)
         elif name in pairs:
             p = index[0]
             if name == "f1":
@@ -673,7 +680,8 @@
                 both(lambda h: scatter(p, h).sent())
     for p in issued:
         both(lambda h: scatter(p, h).sent())
-    both(lambda h: scatter_p(h).sent())
+    for c in range(PARTS):
+        scatter_p(c).sent()
 
 
 def fused(Z, R, T, *args):
@@ -682,7 +690,7 @@
     TOK, DH = mixer_out.shape
     FR, RK = factors.shape
     MR, CW = first_moment.shape
-    NC, HALF = CW // LANES, CW // 2
+    NC, PART = CW // LANES, CW // PARTS
     f32, bf16 = jnp.float32, jnp.bfloat16
     vmem = pl.BlockSpec(memory_space=pltpu.VMEM)
     dma = pltpu.SemaphoreType.DMA
@@ -713,13 +721,13 @@
             pltpu.VMEM((Z, R, FR, RK), bf16),
             pltpu.VMEM((RK, DH), bf16),
             pltpu.VMEM((RK, TOK), bf16),
-            pltpu.VMEM((1, 2, R, Z, MR, HALF), f32),
-            pltpu.VMEM((2, R, Z, MR, HALF), bf16),
-            pltpu.VMEM((2, 2, Z, MR, HALF), bf16),
-            pltpu.VMEM((2, Z, MR, HALF), bf16),
-            pltpu.VMEM((2, Z, MR, HALF), bf16),
-            pltpu.VMEM((2, Z, MR, HALF), bf16),
-            pltpu.VMEM((2, Z, MR, HALF), bf16),
+            pltpu.VMEM((PARTS, 2, R, Z, MR, PART), f32),
+            pltpu.VMEM((PARTS, R, Z, MR, PART), bf16),
+            pltpu.VMEM((PARTS, 2, Z, MR, PART), bf16),
+            pltpu.VMEM((PARTS, Z, MR, PART), bf16),
+            pltpu.VMEM((PARTS, Z, MR, PART), bf16),
+            pltpu.VMEM((PARTS, Z, MR, PART), bf16),
+            pltpu.VMEM((PARTS, Z, MR, PART), bf16),
             pltpu.VMEM((MR, CW), f32),
             pltpu.VMEM((Z, R, MR, CW), bf16),
             pltpu.VMEM((MR, CW), bf16),
@@ -727,8 +735,8 @@
             pltpu.VMEM((N * T, 2, LANES), f32),
             pltpu.VMEM((8, PAIR), f32),
             *pair(NC, 2), *pair(NC), *pair(NC, Z),
-            *pair(2, 2), *pair(2), *pair(2, Z),
-            *pair(NC + 4, Z), *pair(NC + 4, 3), dma((NC + 4, 2)),
+            *pair(PARTS, 2), *pair(PARTS), *pair(PARTS, Z),
+            *pair(NC + 2 + PARTS, Z), *pair(NC + 2 + PARTS, 3), dma((NC + 2 + PARTS, 2)),
             *pair(N * T), dma, dma,
         ],
         compiler_params=pltpu.CompilerParams(
@@ -778,7 +786,7 @@
     def per_device(*args):
         mixer_out, out_grad, factors, weight, first_moment, second_moment = args
         fits = (
-            out_grad.shape[1] % (4 * PAIR) == 0
+            out_grad.shape[1] % (PARTS * PAIR) == 0
             and mixer_out.shape[0] % PAIR == 0
             and mixer_out.shape[1] % PAIR == 0
             and weight.shape[0] % 16 == 0

time: 134 us -> 130 us (0.970)
  Pallas kernels: 133 us -> 129 us
    pallas_call x1, Pallas kernels: 130 us -> 126 us  [fused(): pl.pallas_call(functools.partial(fused_kernel, Z, R, T), out_shape=(pltpu...]
where the time goes in v5:
time: 130 us
  Pallas kernels  129 us (99%)
    pallas_call x1, Pallas kernels, fused(): pl.pallas_call(functools.partial(fused_kernel, Z, R, T), out_shape=(pltpu...  126 us
    pallas_call x1, Pallas kernels, drain_out(): pl.pallas_call(drain_kernel, out_shape=tuple((jax.ShapeDtypeStruct(a.shap...  3.35 us

profile of v5, /device:TPU:0, one launch (start us, length us, event | category | flops | bytes accessed | tf_op | source)
XLA Modules:
  0.0 130.1 jit_solution(7613767312946705653)
XLA Ops:
  0.6 126.1 %shard_map.101 = (f32[96,2048]{1,0:T(8,128)S(1)}, f32[96,2048]{1,0:T(8,128)S(1)}, f32[16,2048]{1,0:T(8,128)S(1)}, f32[16,2048]{1,0:T(8,128)S(1)}, bf16[4,4,96,2048]{3,2,1,0:T(8,128)(2,1)S(1)}) custom-call(bf16[1024,1536]{1,0:T(8,128)(2,1)} %m_hbm.1, bf16[1024,2048]{1,0:T(8,128)(2,1)} %o_hbm.1, bf16[96,256]{1,0:T(8,128)(2,1)} %f_hbm.1, f32[96,2048]{1,0:T(8,128)} %w_hbm.1, ...), custom_call_target="tpu_custom_call" | custom-call | tf_op jit(solution)/shard_map/pallas_call | solution.py:698
  126.7 3.4 %shard_map.102 = (f32[96,2048]{1,0:T(8,128)}, f32[96,2048]{1,0:T(8,128)}, f32[16,2048]{1,0:T(8,128)}, f32[16,2048]{1,0:T(8,128)}, bf16[4,4,96,2048]{3,2,1,0:T(8,128)(2,1)}) custom-call(f32[96,2048]{1,0:T(8,128)S(1)} %get-tuple-element.15.refs_0_, f32[96,2048]{1,0:T(8,128)S(1)} %get-tuple-element.16.refs_1_, f32[16,2048]{1,0:T(8,128)S(1)} %get-tuple-element.17.refs_2_, ...), custom_call_target="tpu_custom_call" | custom-call | tf_op jit(solution)/shard_map/pallas_call | solution.py:117

commit v6 on v5

--- a/solution.py
+++ b/solution.py
@@ -221,7 +221,7 @@
         def first(self, k):
             rr = self.n1 if k else dn
             c = self.c
-            return move(self.s1.at[c, rr], self.r1.at[c, k], self.ts.at[c, k], self.tr.at[c, k], device(z, self.n1, t))
+            return move(self.s1.at[c, rr], self.r1.at[c, k], self.ts.at[c], self.tr.at[c, k], device(z, self.n1, t))
 
         def second(self):
             c = self.c
@@ -230,7 +230,17 @@
         def third(self, zz, src):
             c = self.c
             return move(
-                self.s3.at[c, zz], self.r3.at[c, src], self.vs.at[c, zz], self.vr.at[c, src], device(zz, r, t)
+                self.s3.at[c, zz], self.r3.at[c, src], self.vs.at[c], self.vr.at[c], device(zz, r, t)
+            )
+
+        def thirds(self):
+            every_block = self.r3.at[self.c, pl.ds(0, Z - 1)]
+            return move(every_block, every_block, self.vs.at[self.c], self.vr.at[self.c], device(other(1), r, t))
+
+        def firsts(self):
+            return move(
+                self.r1.at[self.c], self.r1.at[self.c], self.ts.at[self.c], self.tr.at[self.c, 0],
+                device(z, self.n1, t),
             )
 
         def mine(self, rr, zz):
@@ -264,17 +274,16 @@
             put(total(z))
 
         def last(self, get, put):
-            each_z(lambda zz: self.third(zz, zz).wait_recv())
+            self.thirds().wait_recv()
             value = get()
             for e in range(1, Z):
                 value = value + self.r3[self.c, other(e)].astype(f32)
             put(value)
 
         def sent(self):
-            self.first(0).wait_send()
-            self.first(1).wait_send()
+            self.firsts().wait_send()
             self.second().wait_send()
-            each_z(lambda zz: self.third(zz, z).wait_send())
+            self.thirds().wait_send()
 
     class Gather:
         def __init__(self, g, h, ref, cols, rows=slice(None)):
@@ -285,13 +294,13 @@
             place = self.ref.at[src_z, r, self.rows, self.cols]
             return move(
                 place if block is None else block, place,
-                gz_send.at[self.g, zz] if sent is None else sent, gz_recv.at[self.g, src_z], device(zz, r, t),
+                gz_send.at[self.g] if sent is None else sent, gz_recv.at[self.g, src_z], device(zz, r, t),
             )
 
         def beside(self, k, rr):
             place = self.ref.at[:, rr, self.rows, self.cols]
             to = self.n2 if k == 0 else self.n1
-            return move(place, place, gx_send.at[self.g, k], gx_recv.at[self.g, k], device(z, to, t))
+            return move(place, place, gx_send.at[self.g], gx_recv.at[self.g, k], device(z, to, t))
 
         def stage1(self, block=None):
             each_z(lambda zz: self.along(zz, z, block).start())
@@ -301,7 +310,7 @@
             self.along(twin, z).start()
 
         def onward(self, k):
-            return self.along(twin, away + k, None, gf_send.at[self.g, k])
+            return self.along(twin, away + k, None, gf_send.at[self.g])
 
         def forward(self):
             @pl.when(middle)
@@ -318,14 +327,20 @@
                 for k in (0, 1):
                     self.along(twin, away + k).wait_recv()
 
+        def along_sent(self, blocks, sem):
+            place = self.ref.at[pl.ds(0, blocks), r, self.rows, self.cols]
+            move(place, place, sem, gz_recv.at[self.g, twin], device(twin, r, t)).wait_send()
+
+        def beside_sent(self):
+            place = self.ref.at[:, pl.ds(0, 3), self.rows, self.cols]
+            move(place, place, gx_send.at[self.g], gx_recv.at[self.g, 0], device(z, self.n1, t)).wait_send()
+
         def spread_sent(self):
-            self.along(cross, z).wait_send()
-            self.along(twin, z).wait_send()
+            self.along_sent(2, gz_send.at[self.g])
 
             @pl.when(middle)
             def _():
-                for k in (0, 1):
-                    self.onward(k).wait_send()
+                self.along_sent(2, gf_send.at[self.g])
 
         def stage2(self, spread=False):
             if spread:
@@ -345,22 +360,28 @@
             if spread:
                 self.spread_sent()
             else:
-                each_z(lambda zz: self.along(zz, z).wait_send())
-            self.beside(0, r).wait_send()
-            self.beside(1, r).wait_send()
-            self.beside(2, self.n2).wait_send()
+                self.along_sent(Z - 1, gz_send.at[self.g])
+            self.beside_sent()
 
     class ScatterZ(Scatter):
         def far(self, zz, src):
             c = self.c
             return move(
-                self.s1.at[c, :, zz], rz.at[along_z[c], src], self.vs.at[c, zz], self.vr.at[c, src], device(zz, r, t)
+                self.s1.at[c, :, zz], rz.at[along_z[c], src], self.vs.at[c], self.vr.at[c], device(zz, r, t)
             )
+
+        def thirds(self):
+            every_block = rz.at[along_z[self.c], pl.ds(0, Z - 1)]
+            return move(every_block, every_block, self.vs.at[self.c], self.vr.at[self.c], device(other(1), r, t))
+
+        def firsts(self):
+            both_blocks = self.r2.at[self.c, pl.ds(0, 2)]
+            return move(both_blocks, both_blocks, self.ts.at[self.c], self.tr.at[self.c, 0], device(z, self.n1, t))
 
         def first(self, k):
             rr = self.n1 if k else dn
             c = self.c
-            return move(self.s2.at[c, rr], self.r2.at[c, k], self.ts.at[c, k], self.tr.at[c, k], device(z, self.n1, t))
+            return move(self.s2.at[c, rr], self.r2.at[c, k], self.ts.at[c], self.tr.at[c, k], device(z, self.n1, t))
 
         def second(self):
             c = self.c
@@ -370,7 +391,7 @@
             each_z(lambda zz: self.far(zz, z).start())
 
         def stage2(self):
-            each_z(lambda zz: self.far(zz, zz).wait_recv())
+            self.thirds().wait_recv()
 
             def add(rr, carry):
                 total = self.mine(rr, z)
@@ -397,23 +418,30 @@
             put(self.mine(r, z) + self.r2[c, 1].astype(f32) + self.r3[c, 0].astype(f32))
 
         def sent(self):
-            self.first(0).wait_send()
-            self.first(1).wait_send()
+            self.firsts().wait_send()
             self.second().wait_send()
-            each_z(lambda zz: self.far(zz, z).wait_send())
+            self.thirds().wait_send()
 
     class GatherZ(Gather):
         def along(self, zz, src_z, block=None, sent=None):
             place = self.ref.at[src_z, :, :, self.cols]
             return move(
-                place, place, gz_send.at[self.g, zz] if sent is None else sent, gz_recv.at[self.g, src_z],
+                place, place, gz_send.at[self.g] if sent is None else sent, gz_recv.at[self.g, src_z],
                 device(zz, r, t),
             )
+
+        def along_sent(self, blocks, sem):
+            place = self.ref.at[pl.ds(0, blocks), :, :, self.cols]
+            move(place, place, sem, gz_recv.at[self.g, twin], device(twin, r, t)).wait_send()
+
+        def beside_sent(self):
+            place = self.ref.at[z, pl.ds(0, 3), :, self.cols]
+            move(place, place, gx_send.at[self.g], gx_recv.at[self.g, 0], device(z, self.n1, t)).wait_send()
 
         def beside(self, k, rr):
             place = self.ref.at[z, rr, :, self.cols]
             to = self.n2 if k == 0 else self.n1
-            return move(place, place, gx_send.at[self.g, k], gx_recv.at[self.g, k], device(z, to, t))
+            return move(place, place, gx_send.at[self.g], gx_recv.at[self.g, k], device(z, to, t))
 
         def begin(self):
             self.beside(0, r).start()
@@ -431,9 +459,7 @@
         def done(self, spread=True):
             self.gathered()
             self.spread_sent()
-            self.beside(0, r).wait_send()
-            self.beside(1, r).wait_send()
-            self.beside(2, self.n2).wait_send()
+            self.beside_sent()
 
     main_refs = (own, s1, r1, s2, r2, s3, r3)
     main_sems = (t_send, t_recv, u_send, u_recv, v_send, v_recv)
@@ -532,13 +558,11 @@
         for k in (0, 1):
             scatter_p(c).first(k).start()
 
-    def s_copy(p, slot_of):
+    def s_copy(p):
         q = lax.rem(every + p, N * T)
         d = q // T
-        slot = slot_of(q)
         return move(
-            stat, stat_all.at[slot], st_send.at[q], st_recv.at[slot],
-            device(d // R, lax.rem(d, R), lax.rem(q, T)),
+            stat, stat_all.at[every], st_send, st_recv, device(d // R, lax.rem(d, R), lax.rem(q, T))
         )
 
     def fold(value):
@@ -562,17 +586,14 @@
         stat_all[every] = stat[...]
 
         def send(p, carry):
-            s_copy(p, lambda q: every).start()
+            s_copy(p).start()
             return carry
 
         lax.fori_loop(1, N * T, send, 0)
 
     def combine():
-        def wait(p, carry):
-            s_copy(p, lambda q: q).wait()
-            return carry
-
-        lax.fori_loop(1, N * T, wait, 0)
+        arrivals = stat_all.at[pl.ds(0, N * T - 1)]
+        move(arrivals, arrivals, st_send, st_recv, device(z, r, 1 - t)).wait()
         totals = jnp.sum(stat_all[...], axis=0)
         dir_sum = jnp.sum(totals[0:1, :], axis=1, keepdims=True)
         proj_sum = jnp.sum(totals[1:2, :], axis=1, keepdims=True)
@@ -691,6 +712,7 @@
     FR, RK = factors.shape
     MR, CW = first_moment.shape
     NC, PART = CW // LANES, CW // PARTS
+    GC = NC + 2 + PARTS
     f32, bf16 = jnp.float32, jnp.bfloat16
     vmem = pl.BlockSpec(memory_space=pltpu.VMEM)
     dma = pltpu.SemaphoreType.DMA
@@ -734,10 +756,10 @@
             pltpu.VMEM((2, LANES), f32),
             pltpu.VMEM((N * T, 2, LANES), f32),
             pltpu.VMEM((8, PAIR), f32),
-            *pair(NC, 2), *pair(NC), *pair(NC, Z),
-            *pair(PARTS, 2), *pair(PARTS), *pair(PARTS, Z),
-            *pair(NC + 2 + PARTS, Z), *pair(NC + 2 + PARTS, 3), dma((NC + 2 + PARTS, 2)),
-            *pair(N * T), dma, dma,
+            dma((NC,)), dma((NC, 2)), *pair(NC), *pair(NC),
+            dma((PARTS,)), dma((PARTS, 2)), *pair(PARTS), *pair(PARTS),
+            dma((GC,)), dma((GC, Z)), dma((GC,)), dma((GC, 3)), dma((GC,)),
+            dma, dma, dma, dma,
         ],
         compiler_params=pltpu.CompilerParams(
             collective_id=0, has_side_effects=True, vmem_limit_bytes=VMEM_GRANT

time: 130 us -> 127 us (0.977)
  Pallas kernels: 129 us -> 126 us
    pallas_call x1, Pallas kernels: 126 us -> 123 us  [fused(): pl.pallas_call(functools.partial(fused_kernel, Z, R, T), out_shape=(pltpu...]
where the time goes in v6:
time: 127 us
  Pallas kernels  126 us (99%)
    pallas_call x1, Pallas kernels, fused(): pl.pallas_call(functools.partial(fused_kernel, Z, R, T), out_shape=(pltpu...  123 us
    pallas_call x1, Pallas kernels, drain_out(): pl.pallas_call(drain_kernel, out_shape=tuple((jax.ShapeDtypeStruct(a.shap...  3.35 us

profile of v6, /device:TPU:0, one launch (start us, length us, event | category | flops | bytes accessed | tf_op | source)
XLA Modules:
  0.0 127.0 jit_solution(13777244948210977496)
XLA Ops:
  0.6 123.0 %shard_map.101 = (f32[96,2048]{1,0:T(8,128)S(1)}, f32[96,2048]{1,0:T(8,128)S(1)}, f32[16,2048]{1,0:T(8,128)S(1)}, f32[16,2048]{1,0:T(8,128)S(1)}, bf16[4,4,96,2048]{3,2,1,0:T(8,128)(2,1)S(1)}) custom-call(bf16[1024,1536]{1,0:T(8,128)(2,1)} %m_hbm.1, bf16[1024,2048]{1,0:T(8,128)(2,1)} %o_hbm.1, bf16[96,256]{1,0:T(8,128)(2,1)} %f_hbm.1, f32[96,2048]{1,0:T(8,128)} %w_hbm.1, ...), custom_call_target="tpu_custom_call" | custom-call | tf_op jit(solution)/shard_map/pallas_call | solution.py:720
  123.6 3.4 %shard_map.102 = (f32[96,2048]{1,0:T(8,128)}, f32[96,2048]{1,0:T(8,128)}, f32[16,2048]{1,0:T(8,128)}, f32[16,2048]{1,0:T(8,128)}, bf16[4,4,96,2048]{3,2,1,0:T(8,128)(2,1)}) custom-call(f32[96,2048]{1,0:T(8,128)S(1)} %get-tuple-element.15.refs_0_, f32[96,2048]{1,0:T(8,128)S(1)} %get-tuple-element.16.refs_1_, f32[16,2048]{1,0:T(8,128)S(1)} %get-tuple-element.17.refs_2_, ...), custom_call_target="tpu_custom_call" | custom-call | tf_op jit(solution)/shard_map/pallas_call | solution.py:117

commit v7 on v6

--- a/solution.py
+++ b/solution.py
@@ -290,11 +290,11 @@
             self.g, self.ref, self.cols, self.rows = g, ref, cols, rows
             self.n1, self.n2 = near[h]
 
-        def along(self, zz, src_z, block=None, sent=None):
+        def along(self, zz, src_z, block=None, sent=None, got=None):
             place = self.ref.at[src_z, r, self.rows, self.cols]
             return move(
                 place if block is None else block, place,
-                gz_send.at[self.g] if sent is None else sent, gz_recv.at[self.g, src_z], device(zz, r, t),
+                gz_send.at[self.g] if sent is None else sent, gz_recv.at[self.g, src_z if got is None else got], device(zz, r, t),
             )
 
         def beside(self, k, rr):
@@ -303,7 +303,7 @@
             return move(place, place, gx_send.at[self.g], gx_recv.at[self.g, k], device(z, to, t))
 
         def stage1(self, block=None):
-            each_z(lambda zz: self.along(zz, z, block).start())
+            each_z(lambda zz: self.along(zz, z, block, None, 0).start())
 
         def spread(self):
             self.along(cross, z).start()
@@ -346,7 +346,8 @@
             if spread:
                 self.gathered()
             else:
-                each_z(lambda zz: self.along(zz, zz).wait_recv())
+                place = self.ref.at[pl.ds(0, Z - 1), r, self.rows, self.cols]
+                move(place, place, gz_send.at[self.g], gz_recv.at[self.g, 0], device(twin, r, t)).wait_recv()
             self.beside(0, r).start()
             self.beside(1, r).start()
 

time: 127 us -> 127 us (level)
  no operation moved by 1% of the time
where the time goes in v7:
time: 127 us
  Pallas kernels  126 us (99%)
    pallas_call x1, Pallas kernels, fused(): pl.pallas_call(functools.partial(fused_kernel, Z, R, T), out_shape=(pltpu...  123 us
    pallas_call x1, Pallas kernels, drain_out(): pl.pallas_call(drain_kernel, out_shape=tuple((jax.ShapeDtypeStruct(a.shap...  3.35 us

profile of v7, /device:TPU:0, one launch (start us, length us, event | category | flops | bytes accessed | tf_op | source)
XLA Modules:
  0.0 127.0 jit_solution(12619208319366710988)
XLA Ops:
  0.6 123.0 %shard_map.101 = (f32[96,2048]{1,0:T(8,128)S(1)}, f32[96,2048]{1,0:T(8,128)S(1)}, f32[16,2048]{1,0:T(8,128)S(1)}, f32[16,2048]{1,0:T(8,128)S(1)}, bf16[4,4,96,2048]{3,2,1,0:T(8,128)(2,1)S(1)}) custom-call(bf16[1024,1536]{1,0:T(8,128)(2,1)} %m_hbm.1, bf16[1024,2048]{1,0:T(8,128)(2,1)} %o_hbm.1, bf16[96,256]{1,0:T(8,128)(2,1)} %f_hbm.1, f32[96,2048]{1,0:T(8,128)} %w_hbm.1, ...), custom_call_target="tpu_custom_call" | custom-call | tf_op jit(solution)/shard_map/pallas_call | solution.py:721
  123.6 3.4 %shard_map.102 = (f32[96,2048]{1,0:T(8,128)}, f32[96,2048]{1,0:T(8,128)}, f32[16,2048]{1,0:T(8,128)}, f32[16,2048]{1,0:T(8,128)}, bf16[4,4,96,2048]{3,2,1,0:T(8,128)(2,1)}) custom-call(f32[96,2048]{1,0:T(8,128)S(1)} %get-tuple-element.15.refs_0_, f32[96,2048]{1,0:T(8,128)S(1)} %get-tuple-element.16.refs_1_, f32[16,2048]{1,0:T(8,128)S(1)} %get-tuple-element.17.refs_2_, ...), custom_call_target="tpu_custom_call" | custom-call | tf_op jit(solution)/shard_map/pallas_call | solution.py:117
